TPU v7x, 256 devices: a whole 4x4x8 slice. The times are simulated.
256 devices in a mesh: sp: 32 (over z, x), fs: 4 (over y), tp: 2 (over core).
Axes of the slice: x: 4, y: 4, z: 8, core: 2. Of those that a mesh axis runs over, the one named last changes fastest.
Arguments:
- inputs: bfloat16 [4, 8192, 2048], P('fs', ('sp', 'tp')), may hold values from -6 to 6
- norm_gain: float32 [2048], replicated, may hold values from 0.1 to 1.9
- w_glu_value: bfloat16 [2048, 1024], P(None, 'tp'), may hold values from -0.125 to 0.125
- w_glu_gate: bfloat16 [2048, 1024], P(None, 'tp'), may hold values from -0.125 to 0.125
- w_query_one: bfloat16 [2048, 512], P(None, 'tp'), may hold values from -2.5 to 2.5
- w_query_two: bfloat16 [2048, 512], P(None, 'tp'), may hold values from -2.5 to 2.5
- w_key_one: bfloat16 [2048, 512], P(None, 'tp'), may hold values from -2.5 to 2.5
- w_key_two: bfloat16 [2048, 512], P(None, 'tp'), may hold values from -2.5 to 2.5
- w_value: bfloat16 [2048, 1024], P(None, 'tp'), may hold values from -0.125 to 0.125
- conv_kernel: bfloat16 [31, 1024], P(None, 'tp'), may hold values from -1 to 1
- conv_gain: float32 [1024], P('tp'), may hold values from 0.1 to 1.9
- head_gain: float32 [128], replicated, may hold values from 0.1 to 1.9
- lambda_head: float32 [8], P('tp'), may hold values from 0.3 to 0.8
- w_out_conv: bfloat16 [1024, 2048], P('tp', 'fs'), may hold values from -0.125 to 0.125
- w_out_attn: bfloat16 [1024, 2048], P('tp', 'fs'), may hold values from -0.125 to 0.125
Outputs:
- mixed: bfloat16 [4, 8192, 2048], P('fs', ('sp', 'tp'))
- log_sums: float32 [4, 2, 8, 8192], P('fs', None, 'tp', 'sp')
All inputs are finite; a program needn't handle non-finite values.
Results may differ from a plain program's by a relative error of at most 0.013.
Values may be sent and summed in bfloat16 or wider, within the bound.
A program may use at most 128 MiB of HBM per device.

v0:
```python
import math

import jax
import jax.numpy as jnp
from jax import lax
from jax.sharding import PartitionSpec as P

DC = 1024
HD = 64
VD = 128
CW = 31
SEG = 64


NEG_FILL = -1e30
EPSILON = 1e-05
HEAD_SCALE = 0.8


def copy_for_each(x, axis):
    copies = jnp.broadcast_to(x, (lax.axis_size(axis), *x.shape))
    return lax.all_to_all(copies, axis, split_axis=0, concat_axis=0, tiled=True)


def in_order(parts, dim):
    parts = jnp.moveaxis(parts, 0, dim)
    lengths = parts.shape
    return parts.reshape(*lengths[:dim], lengths[dim] * lengths[dim + 1], *lengths[dim + 2 :])


def gathered_copies(x, axis, dim):
    parts = copy_for_each(x, axis)
    return in_order(parts, dim)


def shifted(value, axis, steps):
    count = lax.axis_size(axis)
    initial, last = (max(0, -steps), min(count, count - steps))
    return lax.ppermute(value, axis, [(source, source + steps) for source in range(initial, last)])


def cut_along(x, dim, peers):
    lengths = x.shape
    parts = x.reshape(*lengths[:dim], peers, lengths[dim] // peers, *lengths[dim + 1 :])
    return jnp.moveaxis(parts, dim, 0)


def summed_on_arrival(x, axis, dim):
    peers = lax.axis_size(axis)
    parts = lax.all_to_all(cut_along(x, dim, peers), axis, 0, 0, tiled=True)
    return jnp.sum(parts.astype(jnp.float32), axis=0)


def update(running, queries, key_rows, value_rows, allowed, score_scale):
    row_max, denominator, summed = running
    scores = (
        jnp.einsum("tgrd,kgd->tgrk", queries, key_rows, preferred_element_type=jnp.float32)
        * score_scale
    )
    scores = jnp.where(allowed, scores, NEG_FILL)
    new_max = jnp.maximum(row_max, jnp.max(scores, axis=-1))
    factor = jnp.exp(row_max - new_max)
    weights = jnp.where(allowed, jnp.exp(scores - new_max[..., None]), 0.0)
    denominator = denominator * factor + jnp.sum(weights, axis=-1)
    summed = summed * factor[..., None] + jnp.einsum(
        "tgrk,kgv->tgrv",
        weights.astype(jnp.bfloat16),
        value_rows,
        preferred_element_type=jnp.float32,
    )
    return (new_max, denominator, summed)


def body(
    inputs,
    norm_gain,
    w_glu_value,
    w_glu_gate,
    w_query_one,
    w_query_two,
    w_key_one,
    w_key_two,
    w_value,
    conv_kernel,
    conv_gain,
    head_gain,
    lambda_head,
    w_out_conv,
    w_out_attn,
):
    weight_list = (w_glu_value, w_glu_gate, w_query_one, w_query_two, w_key_one, w_key_two, w_value)
    rows_f = gathered_copies(inputs, "tp", 1)[0].astype(jnp.float32)
    normed = (
        rows_f * lax.rsqrt(jnp.mean(rows_f * rows_f, axis=-1, keepdims=True) + EPSILON) * norm_gain
    ).astype(jnp.bfloat16)
    outputs = [
        jnp.dot(normed, weight, preferred_element_type=jnp.float32).astype(jnp.bfloat16)
        for weight in weight_list
    ]
    projected = jnp.concatenate(outputs, axis=-1)[None][0]
    tok_rows = projected.shape[0]
    conv_local = w_glu_value.shape[1]
    query_local = w_query_one.shape[1]
    key_local = w_key_one.shape[1]
    bounds = [conv_local, conv_local, query_local, query_local, key_local, key_local]
    pieces_out = []
    offset = 0
    for span in bounds:
        pieces_out.append(projected[:, offset : offset + span])
        offset = offset + span
    pieces_out.append(projected[:, offset:])
    glu_value, glu_gate, query_one, query_two, key_one, key_two, values = pieces_out
    gated = (glu_value.astype(jnp.float32) * jax.nn.sigmoid(glu_gate.astype(jnp.float32))).astype(
        jnp.bfloat16
    )
    earlier = shifted(gated[tok_rows - (CW - 1) :], "sp", 1)
    extended = jnp.concatenate([earlier, gated], axis=0).astype(jnp.float32)
    kernel_f = conv_kernel.astype(jnp.float32)
    convolved = jnp.zeros((tok_rows, conv_local), jnp.float32)
    for tap_index in range(CW):
        convolved = (
            convolved + kernel_f[tap_index][None, :] * extended[tap_index : tap_index + tok_rows]
        )
    row_sums, row_squares = lax.psum(
        (jnp.sum(convolved, axis=-1), jnp.sum(convolved * convolved, axis=-1)), "tp"
    )
    row_mean = (row_sums / DC)[:, None]
    row_square = (row_squares / DC)[:, None]
    conv_out = jax.nn.silu(
        (convolved - row_mean) * lax.rsqrt(row_square - row_mean * row_mean + EPSILON) * conv_gain
    ).astype(jnp.bfloat16)
    kv_local = key_local // HD
    heads_local = query_local // HD
    group = heads_local // kv_local
    query_one_r = query_one.reshape(tok_rows, kv_local, group, HD)
    query_two_r = query_two.reshape(tok_rows, kv_local, group, HD)
    packed = jnp.concatenate([key_one, key_two, values], axis=-1)
    my_start = lax.axis_index("sp") * tok_rows
    query_pos = my_start + lax.iota(jnp.int32, tok_rows)
    score_scale = HD ** (-0.5)
    max_init = jnp.full((tok_rows, kv_local, group), NEG_FILL, jnp.float32)
    sum_init = jnp.zeros((tok_rows, kv_local, group), jnp.float32)
    pooled_init = jnp.zeros((tok_rows, kv_local, group, VD), jnp.float32)
    initial = (max_init, sum_init, pooled_init, max_init, sum_init, pooled_init)
    running = initial
    pieces = lax.all_gather(packed, "sp", axis=0, tiled=True)
    row_count = pieces.shape[0]
    block_rows = math.gcd(row_count, 512)
    block_count = row_count // block_rows
    key_one_b = pieces[:, :key_local].reshape(block_count, block_rows, kv_local, HD)
    key_two_b = pieces[:, key_local : 2 * key_local].reshape(block_count, block_rows, kv_local, HD)
    value_b = pieces[:, 2 * key_local :].reshape(block_count, block_rows, kv_local, VD)

    def advance(status, block):
        key_one_rows, key_two_rows, value_rows, block_index = block
        key_pos = block_index * block_rows + lax.iota(jnp.int32, block_rows)
        allowed = ((key_pos // SEG)[None, :] <= (query_pos // SEG)[:, None]) & (key_pos >= 0)[
            None, :
        ]
        allowed = allowed[:, None, None, :]
        first = update(status[:3], query_one_r, key_one_rows, value_rows, allowed, score_scale)
        second = update(status[3:], query_two_r, key_two_rows, value_rows, allowed, score_scale)
        return (first + second, None)

    running, _ = lax.scan(
        advance, running, (key_one_b, key_two_b, value_b, jnp.arange(block_count, dtype=jnp.int32))
    )
    max_one, sum_one, pooled_one, max_two, sum_two, pooled_two = running
    lambda_local = lambda_head.reshape(kv_local, group)
    head_out = pooled_one / sum_one[..., None] - lambda_local[None, :, :, None] * (
        pooled_two / sum_two[..., None]
    )
    head_out = (
        head_out
        * lax.rsqrt(jnp.mean(head_out * head_out, axis=-1, keepdims=True) + EPSILON)
        * head_gain
        * HEAD_SCALE
    )
    attn_out = head_out.astype(jnp.bfloat16).reshape(tok_rows, heads_local * VD)
    log_pair = jnp.stack([max_one + jnp.log(sum_one), max_two + jnp.log(sum_two)], axis=0).reshape(
        2, tok_rows, heads_local
    )
    log_sums = jnp.transpose(log_pair, (0, 2, 1))[None]
    out_conv_cols, out_attn_cols = (
        lax.all_gather(w_out_conv, "fs", axis=1, tiled=True),
        lax.all_gather(w_out_attn, "fs", axis=1, tiled=True),
    )
    mixed = summed_on_arrival(
        (
            jnp.dot(conv_out, out_conv_cols, preferred_element_type=jnp.float32)
            + jnp.dot(attn_out, out_attn_cols, preferred_element_type=jnp.float32)
        ).astype(jnp.bfloat16),
        "tp",
        0,
    )
    return (mixed.astype(jnp.bfloat16)[None], log_sums)


def solution(mesh):
    return jax.shard_map(
        body,
        mesh=mesh,
        in_specs=(
            P("fs", ("sp", "tp"), None),
            P(),
            P(None, "tp"),
            P(None, "tp"),
            P(None, "tp"),
            P(None, "tp"),
            P(None, "tp"),
            P(None, "tp"),
            P(None, "tp"),
            P(None, "tp"),
            P("tp"),
            P(),
            P("tp"),
            P("tp", "fs"),
            P("tp", "fs"),
        ),
        out_specs=(P("fs", ("sp", "tp"), None), P("fs", None, "tp", "sp")),
        check_vma=False,
    )
```

profile of v0, /device:TPU:1, one launch (start us, length us, event | category | flops | bytes accessed | tf_op | source)
XLA Modules:
  0.0 520.0 jit_solution(15211451502553516199)
XLA Ops:
  9.1 7.4 %all_to_all.10 = bf16[2,1,128,2048]{3,2,1,0:T(8,128)(2,1)S(1)} all-to-all(bf16[2,1,128,2048]{3,2,1,0:T(8,128)(2,1)S(1)} %broadcast_in_dim.73), channel_id=1, replica_groups=mesh['sp'=32,'fs'=4,'tp'=2] {'tp'}, dimensions={0} | all-to-all | bytes 2097152 | tf_op jit(solution)/shard_map/all_to_all | solution.py:22
  35.8 11.0 %all-gather.4.cloned.1.call-done = bf16[512,2048]{1,0:T(8,128)(2,1)} async-done(((bf16[512,512]{1,0:T(8,128)(2,1)}), bf16[512,2048]{1,0:T(8,128)(2,1)}) %all-gather.4.cloned.1.call-update) | async-done | bytes 2097168 | tf_op jit(solution)/shard_map/all_gather | solution.py:185
  46.8 3.8 fusion.94
  50.6 137.9 %all-gather.6.cloned.1.call-done = bf16[8192,1024]{1,0:T(8,128)(2,1)} async-done(((bf16[256,1024]{1,0:T(8,128)(2,1)}), bf16[8192,1024]{1,0:T(8,128)(2,1)}) %all-gather.6.cloned.1.call-update) | async-done | bytes 16777232 | tf_op jit(solution)/shard_map/all_gather | solution.py:146
  188.6 5.8 %fusion.102 = (bf16[8192,256]{1,0:T(8,128)(2,1)}, bf16[8192,256]{1,0:T(8,128)(2,1)}) fusion(bf16[8192,1024]{1,0:T(8,128)(2,1)} %all-gather.6.cloned.1.call-done), kind=kLoop, calls=%fused_computation.182 | loop fusion | bytes 16777216 | tf_op jit(solution)/shard_map/slice | solution.py:151
  194.3 13.0 %reshape.315 = bf16[16,512,4,64]{3,2,1,0:T(4,128)(2,1)} reshape(bf16[8192,256]{1,0:T(8,128)(2,1)} %get-tuple-element.457) | data formatting | bytes 8388608 | tf_op jit(solution)/shard_map/reshape | solution.py:150
  207.3 12.7 %copy.39 = bf16[16,512,4,64]{1,3,2,0:T(8,128)(2,1)} copy(bf16[16,512,4,64]{3,2,1,0:T(4,128)(2,1)} %reshape.315) | data formatting | bytes 8388608
  220.0 12.9 %reshape.316 = bf16[16,512,4,64]{3,2,1,0:T(4,128)(2,1)} reshape(bf16[8192,256]{1,0:T(8,128)(2,1)} %get-tuple-element.456) | data formatting | bytes 8388608 | tf_op jit(solution)/shard_map/reshape | solution.py:151
  233.0 12.7 %copy.41 = bf16[16,512,4,64]{1,3,2,0:T(8,128)(2,1)} copy(bf16[16,512,4,64]{3,2,1,0:T(4,128)(2,1)} %reshape.316) | data formatting | bytes 8388608
  245.7 7.1 %slice.328 = bf16[8192,512]{1,0:T(8,128)(2,1)} slice(bf16[8192,1024]{1,0:T(8,128)(2,1)} %all-gather.6.cloned.1.call-done), slice={[0:8192], [512:1024]} | slice | bytes 16777216 | tf_op jit(solution)/shard_map/slice | solution.py:152
  252.8 12.6 %reshape.296 = bf16[16,512,4,128]{3,2,1,0:T(4,128)(2,1)} reshape(bf16[8192,512]{1,0:T(8,128)(2,1)} %slice.328) | data formatting | bytes 16777216 | tf_op jit(solution)/shard_map/reshape | solution.py:152
  265.4 233.8 %while.26 = (s32[]{:T(128)}, f32[256,4,1]{0,1,2:T(4,128)S(1)}, f32[256,4,1]{0,1,2:T(4,128)}, f32[256,4,1,128]{0,3,1,2:T(8,128)}, f32[256,4,1]{0,1,2:T(4,128)S(1)...) while((s32[]{:T(128)}, f32[256,4,1]{0,1,2:T(4,128)S(1)}, ...), condition=%wide.region_10.11_spmd.clone.clone.clone, body=%wide.region_5.10_spmd.clone.clone.clone.sunk | while | flops 417359360 | bytes 34155988 | solution.py:165
  273.5 3.1 fusion.151
  288.0 3.2 fusion.151
  302.6 3.2 fusion.151
  312.0 3.1 fusion.146
  317.2 3.2 fusion.151
  331.9 3.2 fusion.151
  341.3 3.1 fusion.146
  346.5 3.2 fusion.151
  361.1 3.2 fusion.151
  375.7 3.2 fusion.151
  390.3 3.2 fusion.151
  405.0 3.2 fusion.151
  419.6 3.2 fusion.151
  434.2 3.2 fusion.151
  448.8 3.2 fusion.151
  463.4 3.2 fusion.151
  478.0 3.2 fusion.151
  492.7 3.2 fusion.151
  501.4 4.1 fusion.53
  505.5 5.1 all-to-all-start.1
  (642 shorter events, 191.2 us)
Async XLA Ops:
  7.2 13.1 %copy-start = (bf16[2048,512]{1,0:T(8,128)(2,1)S(1)}, bf16[2048,512]{1,0:T(8,128)(2,1)}, u32[]{:S(2)}) copy-start(bf16[2048,512]{1,0:T(8,128)(2,1)} %param.25) | copy-start | bytes 6291460
  7.2 39.6 %all-gather.4.cloned.1.call-start = ((), (), s32[]{:S(2)}) async-start(), calls=%async_computation.2 | async-start | bytes 2621440 | tf_op jit(solution)/shard_map/all_gather | solution.py:185
  7.9 180.7 %all-gather.6.cloned.1.call-start = ((), (), s32[]{:S(2)}) async-start(), calls=%async_computation.3 | async-start | bytes 17301504 | tf_op jit(solution)/shard_map/all_gather | solution.py:146
  8.0 8.9 %copy-start.17 = (f32[2048]{0:T(1024)S(1)}, f32[2048]{0:T(1024)}, u32[]{:S(2)}) copy-start(f32[2048]{0:T(1024)} %param.18) | copy-start | bytes 24580
  21.9 479.4 %all-gather.8.cloned.1.call-start = ((), (), s32[]{:S(2)}) async-start(), calls=%async_computation.4 | async-start | bytes 2621440 | tf_op jit(solution)/shard_map/all_gather | solution.py:186
  25.9 3.4 copy-start.7
  25.9 4.1 collective-permute-start
  30.1 16.7 %copy-start.18 = (f32[512]{0:T(512)S(1)}, f32[512]{0:T(512)}, u32[]{:S(2)}) copy-start(f32[512]{0:T(512)} %param.27) | copy-start | bytes 6148
  265.4 5.9 %copy-start.19 = (s32[16]{0:T(128)}, s32[16]{0:T(128)S(1)}, u32[]{:S(2)}) copy-start(s32[16]{0:T(128)S(1)} %get-tuple-element.641) | copy-start | bytes 196 | tf_op jit(solution)/shard_map/while
  279.9 5.9 %copy-start.19 = (s32[16]{0:T(128)}, s32[16]{0:T(128)S(1)}, u32[]{:S(2)}) copy-start(s32[16]{0:T(128)S(1)} %get-tuple-element.641) | copy-start | bytes 196 | tf_op jit(solution)/shard_map/while
  294.5 5.9 %copy-start.19 = (s32[16]{0:T(128)}, s32[16]{0:T(128)S(1)}, u32[]{:S(2)}) copy-start(s32[16]{0:T(128)S(1)} %get-tuple-element.641) | copy-start | bytes 196 | tf_op jit(solution)/shard_map/while
  302.6 3.2 copy-start.8
  309.1 5.9 %copy-start.19 = (s32[16]{0:T(128)}, s32[16]{0:T(128)S(1)}, u32[]{:S(2)}) copy-start(s32[16]{0:T(128)S(1)} %get-tuple-element.641) | copy-start | bytes 196 | tf_op jit(solution)/shard_map/while
  323.8 5.9 %copy-start.19 = (s32[16]{0:T(128)}, s32[16]{0:T(128)S(1)}, u32[]{:S(2)}) copy-start(s32[16]{0:T(128)S(1)} %get-tuple-element.641) | copy-start | bytes 196 | tf_op jit(solution)/shard_map/while
  331.8 3.2 copy-start.8
  338.4 5.9 %copy-start.19 = (s32[16]{0:T(128)}, s32[16]{0:T(128)S(1)}, u32[]{:S(2)}) copy-start(s32[16]{0:T(128)S(1)} %get-tuple-element.641) | copy-start | bytes 196 | tf_op jit(solution)/shard_map/while
  353.0 5.9 %copy-start.19 = (s32[16]{0:T(128)}, s32[16]{0:T(128)S(1)}, u32[]{:S(2)}) copy-start(s32[16]{0:T(128)S(1)} %get-tuple-element.641) | copy-start | bytes 196 | tf_op jit(solution)/shard_map/while
  361.1 3.2 copy-start.8
  367.6 5.9 %copy-start.19 = (s32[16]{0:T(128)}, s32[16]{0:T(128)S(1)}, u32[]{:S(2)}) copy-start(s32[16]{0:T(128)S(1)} %get-tuple-element.641) | copy-start | bytes 196 | tf_op jit(solution)/shard_map/while
  382.2 5.9 %copy-start.19 = (s32[16]{0:T(128)}, s32[16]{0:T(128)S(1)}, u32[]{:S(2)}) copy-start(s32[16]{0:T(128)S(1)} %get-tuple-element.641) | copy-start | bytes 196 | tf_op jit(solution)/shard_map/while
  390.3 3.2 copy-start.8
  396.8 5.9 %copy-start.19 = (s32[16]{0:T(128)}, s32[16]{0:T(128)S(1)}, u32[]{:S(2)}) copy-start(s32[16]{0:T(128)S(1)} %get-tuple-element.641) | copy-start | bytes 196 | tf_op jit(solution)/shard_map/while
  411.5 5.9 %copy-start.19 = (s32[16]{0:T(128)}, s32[16]{0:T(128)S(1)}, u32[]{:S(2)}) copy-start(s32[16]{0:T(128)S(1)} %get-tuple-element.641) | copy-start | bytes 196 | tf_op jit(solution)/shard_map/while
  426.1 5.9 %copy-start.19 = (s32[16]{0:T(128)}, s32[16]{0:T(128)S(1)}, u32[]{:S(2)}) copy-start(s32[16]{0:T(128)S(1)} %get-tuple-element.641) | copy-start | bytes 196 | tf_op jit(solution)/shard_map/while
  440.7 5.9 %copy-start.19 = (s32[16]{0:T(128)}, s32[16]{0:T(128)S(1)}, u32[]{:S(2)}) copy-start(s32[16]{0:T(128)S(1)} %get-tuple-element.641) | copy-start | bytes 196 | tf_op jit(solution)/shard_map/while
  455.3 5.9 %copy-start.19 = (s32[16]{0:T(128)}, s32[16]{0:T(128)S(1)}, u32[]{:S(2)}) copy-start(s32[16]{0:T(128)S(1)} %get-tuple-element.641) | copy-start | bytes 196 | tf_op jit(solution)/shard_map/while
  469.9 5.9 %copy-start.19 = (s32[16]{0:T(128)}, s32[16]{0:T(128)S(1)}, u32[]{:S(2)}) copy-start(s32[16]{0:T(128)S(1)} %get-tuple-element.641) | copy-start | bytes 196 | tf_op jit(solution)/shard_map/while
  484.6 5.9 %copy-start.19 = (s32[16]{0:T(128)}, s32[16]{0:T(128)S(1)}, u32[]{:S(2)}) copy-start(s32[16]{0:T(128)S(1)} %get-tuple-element.641) | copy-start | bytes 196 | tf_op jit(solution)/shard_map/while
  501.4 12.1 %copy-start.1 = (bf16[2048,512]{1,0:T(8,128)(2,1)S(1)}, bf16[2048,512]{1,0:T(8,128)(2,1)}, u32[]{:S(2)}) copy-start(bf16[2048,512]{1,0:T(8,128)(2,1)} %param.25) | copy-start | bytes 6291460
  505.5 5.1 copy-start.12
  505.5 5.1 copy-start.15
  505.5 6.9 %all-to-all-start.1 = ((bf16[2,128,2048]{2,1,0:T(8,128)(2,1)}), bf16[2,128,2048]{2,1,0:T(8,128)(2,1)S(1)}, u32[]{:S(2)}, u32[]{:S(2)}) async-start(bf16[2,128,2048]{2,1,0:T(8,128)(2,1)} %bitcast.205), calls=%async_computation.1 | async-start | bytes 2097152 | tf_op jit(solution)/shard_map/all_to_all | solution.py:50
  (129 other events, 169.8 us)
Sparse Core Ops, SparseCore 0:
  9.8 36.9 all-gather.3
  49.4 139.1 all-gather.5
  190.4 30.9 all-gather.7
where the time goes:
time: 524 us; the launch traced here: 520 us
  waiting for transfers between devices  151 us (29%)
  matrix products  151 us (29%)
  local copies, waits for them, and re-layouts  137 us (26%)
  other arithmetic  39 us (7%)
  between operations  14.1 us (3%)
  loops' own time  11.2 us (2%)
  blocking collectives  10.4 us (2%)
  starting transfers between devices  6.79 us (1%)
    all_gather x1, waiting for transfers between devices, body(): pieces = lax.all_gather(packed, 'sp', axis=0, tiled=True)  138 us
    dot_general x32, matrix products, update(): jnp.einsum('tgrd,kgd->tgrk', queries, key_rows, preferred_element_type=jn...  71.9 us
    dot_general x32, matrix products, update(): jnp.einsum('tgrk,kgv->tgrv', weights.astype(jnp.bfloat16), value_rows, pr...  62.8 us
    dynamic_slice x48, local copies, waits for them, and re-layouts, body(): lax.scan(advance, running, (key_one_b, key_two_b, value_b, jnp.arange(blo...  34 us
    unnamed x26, local copies, waits for them, and re-layouts  26.8 us
    while x320, local copies, waits for them, and re-layouts  23 us
    reduce_sum x16, other arithmetic, update(): denominator = denominator * factor + jnp.sum(weights, axis=-1)  16.5 us
    reshape x1, local copies, waits for them, and re-layouts, body(): pieces[:, :key_local].reshape(block_count, block_rows, kv_local, HD)  13 us
  transfers between devices with their start and end apart: 5, of which 3 were waited for; matrix products, arithmetic and copies ran while one was open for 57% of the time, Pallas kernels for 0%

commit v1 on v0

v1 whole, which is shorter than its diff:
```python
import jax
import jax.numpy as jnp
from jax import lax
from jax.experimental import pallas as pl
from jax.experimental.pallas import tpu as pltpu
from jax.sharding import PartitionSpec as P

D = 2048
DC = 1024
HD = 64
CW = 31
NZ = 8
NX = 4
NY = 4
HALF = 128
NEG_FILL = -1e30
EPSILON = 1e-05
HEAD_SCALE = 0.8
MESH = pl.DeviceIdType.MESH
F32 = jnp.float32
BF16 = jnp.bfloat16
Z_ORDER = (0, 1, 7, 2, 6, 3, 5, 4)


def remote(src, dst, send_sem, recv_sem, device):
    return pltpu.make_async_remote_copy(
        src_ref=src,
        dst_ref=dst,
        send_sem=send_sem,
        recv_sem=recv_sem,
        device_id=device,
        device_id_type=MESH,
    )


def kernel(
    x_ref,
    gain_ref,
    ck_ref,
    cg_ref,
    hg_ref,
    lam_ref,
    wgv_hbm,
    wgg_hbm,
    wq1_hbm,
    wq2_hbm,
    wk1_hbm,
    wk2_hbm,
    wv_hbm,
    woc_hbm,
    woa_hbm,
    out_ref,
    log_ref,
    wgv,
    wgg,
    wq1,
    wq2,
    wk1,
    wk2,
    wv,
    normed,
    kv_send,
    q_send,
    kv_buf,
    q_raw,
    qs,
    gated_ext,
    halo_send,
    halo_recv,
    convd,
    sums_send,
    sums_recv,
    conv_full,
    conv_send,
    m_buf,
    acc,
    ret_send,
    attn_buf,
    lsend,
    log_buf,
    lam_recv,
    w_buf,
    acc_out,
    load_sem,
    norm_sem,
    kv_ss,
    q_ss,
    kv_rs,
    q_rs,
    xs_ss,
    xs_rs,
    d_ss,
    d_rs,
    halo_sem,
    sums_sem,
    cx_sem,
    lam_sem,
    ret_ss,
    ret_rs,
    log_ss,
    log_rs,
    w_ss,
    w_rs,
    wd_ss,
    wd_rs,
    own_sem,
):
    me = lax.axis_index("sp")
    y = lax.axis_index("fs")
    c = lax.axis_index("tp")
    z, x = me // NX, me % NX
    other = 1 - c
    xr, xl, xo = (x + 1) % NX, (x + 3) % NX, (x + 2) % NX
    yr, yl, yo = (y + 1) % NY, (y + 3) % NY, (y + 2) % NY
    src_tp = z // 4
    partner = {"tp": other}
    right = {"sp": z * NX + xr}
    left = {"sp": z * NX + xl}
    up = {"fs": yr}
    down = {"fs": yl}
    following = {"sp": (me + 1) % (NZ * NX)}
    preceding = {"sp": (me + NZ * NX - 1) % (NZ * NX)}
    pending = []

    loads = []
    for index, (src, dst) in enumerate(
        ((wv_hbm, wv), (wk1_hbm, wk1), (wk2_hbm, wk2), (wq1_hbm, wq1), (wq2_hbm, wq2),
         (wgv_hbm, wgv), (wgg_hbm, wgg))
    ):
        loads.append(pltpu.make_async_copy(src, dst, load_sem.at[index]))
        loads[-1].start()

    barrier = pltpu.get_barrier_semaphore()
    for device in (partner, right, left, up, down, following, preceding):
        pl.semaphore_signal(barrier, inc=1, device_id=device, device_id_type=MESH)
    for step in range(1, NZ):
        for core in range(2):
            pl.semaphore_signal(
                barrier,
                inc=1,
                device_id={"sp": ((z + step) % NZ) * NX + x, "tp": core},
                device_id_type=MESH,
            )

    my_rows = pl.multiple_of(c * HALF, HALF)
    for part in range(4):
        rows_f = x_ref[part * 32 : part * 32 + 32, :].astype(F32)
        scale = lax.rsqrt(jnp.mean(rows_f * rows_f, axis=-1, keepdims=True) + EPSILON)
        normed[pl.ds(my_rows + part * 32, 32), :] = (rows_f * scale * gain_ref[...]).astype(BF16)

    pl.semaphore_wait(barrier, 7 + 2 * (NZ - 1))

    mine = normed.at[pl.ds(my_rows, HALF), :]
    norm_copy = remote(mine, mine, norm_sem.at[0], norm_sem.at[1], partner)
    norm_copy.start()
    lam_copy = remote(lam_ref, lam_recv, lam_sem.at[0], lam_sem.at[1], partner)
    lam_copy.start()
    pending.append(lam_copy)

    w_hbm = (woc_hbm, woa_hbm)
    own_w = []
    for kind in range(2):
        own = pltpu.make_async_copy(w_hbm[kind], w_buf.at[y, c, kind], own_sem.at[kind])
        own.start()
        own_w.append(own)
    for kind in (0, 1):
        copy = remote(w_hbm[kind], w_buf.at[y, c, kind], w_ss.at[0, kind], w_rs.at[0, kind], up)
        copy.start()
        pending.append(copy)
        copy = remote(
            w_hbm[1 - kind], w_buf.at[y, c, 1 - kind], w_ss.at[1, 1 - kind], w_rs.at[1, 1 - kind], down
        )
        copy.start()
        pending.append(copy)

    norm_copy.wait()

    def project(load, weight):
        load.wait()
        return jnp.dot(normed[...], weight[...], preferred_element_type=F32)

    lane = lax.broadcasted_iota(jnp.int32, (2 * HALF, 128), 1)
    low = lane < HD

    def head_pair(one, two, head):
        pair = slice((head // 2) * 128, (head // 2) * 128 + 128)
        first, second = one[:, pair], two[:, pair]
        if head % 2 == 0:
            return jnp.where(low, first, pltpu.roll(second, HD, 1))
        return jnp.where(low, pltpu.roll(first, HD, 1), second)

    values = project(loads[0], wv)
    for head in range(4):
        for half in range(2):
            kv_send[head, half, :, 128:256] = values[
                half * HALF : half * HALF + HALF, head * 128 : head * 128 + 128
            ].astype(BF16)
    key_one = project(loads[1], wk1)
    key_two = project(loads[2], wk2)
    for head in range(4):
        both = head_pair(key_one, key_two, head).astype(BF16)
        for half in range(2):
            kv_send[head, half, :, 0:128] = both[half * HALF : half * HALF + HALF]
    query_one = project(loads[3], wq1)
    query_two = project(loads[4], wq2)
    for head in range(4):
        both = (head_pair(query_one, query_two, head) * (HD**-0.5)).astype(BF16)
        for half in range(2):
            q_send[head, half] = both[half * HALF : half * HALF + HALF]

    def slot(zs, xs, cs):
        return kv_buf.at[zs, pl.ds(pl.multiple_of((xs * 2 + cs) * HALF, HALF), HALF), :]

    def slot_half(zs, xs, cs, part):
        start = pl.multiple_of((xs * 2 + cs) * HALF + part * (HALF // 2), HALF // 2)
        return kv_buf.at[zs, pl.ds(start, HALF // 2), :]

    z_sends = []
    for step in range(4):
        head = (z + step) % 4
        target = 4 * c + head
        for core in range(2):
            index = step * 2 + core
            device = {"sp": target * NX + x, "tp": core}
            kv_copy = remote(
                kv_send.at[head, core], slot(z, x, core), kv_ss.at[index], kv_rs.at[z], device
            )
            q_copy = remote(q_send.at[head, core], q_raw.at[z], q_ss.at[index], q_rs.at[z], device)
            if step == 0:
                away = jnp.logical_not((target == z) & (c == core))
            else:
                away = jnp.logical_not((target == z) & (c == core))
            z_sends.append((away, kv_copy, q_copy))

            @pl.when(away)
            def _(kv_copy=kv_copy, q_copy=q_copy):
                kv_copy.start()
                q_copy.start()

    own_head = z % 4
    local = src_tp == c

    @pl.when(local)
    def _():
        kv_buf[z, pl.ds(pl.multiple_of((x * 2 + c) * HALF, HALF), HALF), :] = kv_send[own_head, c]
        q_raw[z] = q_send[own_head, c]

    glu_value = project(loads[5], wgv).astype(BF16).astype(F32)
    glu_gate = project(loads[6], wgg).astype(BF16).astype(F32)
    gated = (glu_value * jax.nn.sigmoid(glu_gate)).astype(BF16)
    halo_send[...] = gated[2 * HALF - 32 :]
    gated_ext[32:, :] = gated.astype(F32)
    halo_copy = remote(halo_send, halo_recv, halo_sem.at[0], halo_sem.at[1], following)
    halo_copy.start()
    pending.append(halo_copy)

    taps = ck_ref[...]

    def conv_chunk(part):
        base = part * 32
        total = None
        for shift in range(8):
            partial = None
            span = 32 if shift == 0 else 40
            for group in range(5):
                tap = 8 * group + shift - 2
                if tap < 0 or tap >= CW:
                    continue
                term = taps[tap : tap + 1, :] * gated_ext[base + 8 * group : base + 8 * group + span, :]
                partial = term if partial is None else partial + term
            moved = partial[shift : shift + 32, :]
            total = moved if total is None else total + moved
        convd[base : base + 32, :] = total
        sums = jnp.sum(total, axis=-1, keepdims=True)
        squares = jnp.sum(total * total, axis=-1, keepdims=True)
        sums_send[base : base + 32, :] = jnp.where(low[:32], sums, squares)

    def stage_one(zs):
        copies = (
            remote(slot(zs, x, c), slot(zs, x, c), xs_ss.at[0, zs], xs_rs.at[0, zs], right),
            remote(slot(zs, x, c), slot(zs, x, c), xs_ss.at[1, zs], xs_rs.at[1, zs], left),
            remote(slot(zs, x, c), slot(zs, x, c), d_ss.at[0, zs], d_rs.at[0, zs], partner),
        )

        @pl.when(jnp.logical_not((zs == z) & local))
        def _():
            remote(slot(zs, x, c), slot(zs, x, c), kv_ss.at[0], kv_rs.at[zs], partner).wait_recv()

        for copy in copies:
            copy.start()
        pending.extend(copies)

    def stage_two(zs):
        remote(slot(zs, xl, c), slot(zs, xl, c), xs_ss.at[0, zs], xs_rs.at[0, zs], right).wait_recv()
        copies = (
            remote(
                slot_half(zs, xl, c, 0), slot_half(zs, xl, c, 0), xs_ss.at[2, zs], xs_rs.at[2, zs], right
            ),
            remote(slot(zs, xl, c), slot(zs, xl, c), d_ss.at[1, zs], d_rs.at[1, zs], partner),
        )
        for copy in copies:
            copy.start()
        pending.extend(copies)
        remote(slot(zs, xr, c), slot(zs, xr, c), xs_ss.at[1, zs], xs_rs.at[1, zs], left).wait_recv()
        copies = (
            remote(
                slot_half(zs, xr, c, 1), slot_half(zs, xr, c, 1), xs_ss.at[3, zs], xs_rs.at[3, zs], left
            ),
            remote(slot(zs, xr, c), slot(zs, xr, c), d_ss.at[2, zs], d_rs.at[2, zs], partner),
        )
        for copy in copies:
            copy.start()
        pending.extend(copies)

    def stage_three(zs):
        for part in range(2):
            remote(
                slot_half(zs, xo, c, part),
                slot_half(zs, xo, c, part),
                xs_ss.at[2 + part, zs],
                xs_rs.at[2 + part, zs],
                right,
            ).wait_recv()
        copy = remote(slot(zs, xo, c), slot(zs, xo, c), d_ss.at[3, zs], d_rs.at[3, zs], partner)
        copy.start()
        pending.append(copy)

    def w_wait(kind, side):
        source = yl if side == 0 else yr
        ref = w_buf.at[source, c, kind]
        remote(ref, ref, w_ss.at[side, kind], w_rs.at[side, kind], up).wait_recv()
        return ref

    def w_share(source, kind, relation):
        ref = w_buf.at[source, c, kind]
        copy = remote(ref, ref, wd_ss.at[relation, kind], wd_rs.at[relation, kind], partner)
        copy.start()
        return copy

    order = [(z + offset) % NZ for offset in Z_ORDER]
    for step in range(NZ + 2):
        if step < NZ:
            stage_one(order[step])
        if step == 0:
            halo_copy.wait_recv()
            rows = halo_recv[...].astype(F32)
            gated_ext[0:32, :] = jnp.where(me == 0, jnp.zeros_like(rows), rows)
        if 0 <= step - 1 < NZ:
            stage_two(order[step - 1])
        if 0 <= step - 2 < NZ:
            stage_three(order[step - 2])
        if step < NZ:
            conv_chunk(step)
        if step == NZ:
            sums_copy = remote(sums_send, sums_recv, sums_sem.at[0], sums_sem.at[1], partner)
            sums_copy.start()
            pending.append(sums_copy)

    for kind in range(2):
        own_w[kind].wait()
        pending.append(w_share(y, kind, 0))
    ref = w_wait(0, 0)
    copy = remote(ref, ref, w_ss.at[2, 0], w_rs.at[2, 0], up)
    copy.start()
    pending.append(copy)
    pending.append(w_share(yl, 0, 1))
    ref = w_wait(1, 1)
    copy = remote(ref, ref, w_ss.at[2, 1], w_rs.at[2, 1], down)
    copy.start()
    pending.append(copy)
    pending.append(w_share(yr, 1, 2))

    sums_copy.wait_recv()
    lam_copy.wait_recv()
    for half in range(2):
        rows = slice(half * HALF, half * HALF + HALF)
        row_sums = sums_send[rows, :] + sums_recv[rows, :]
        mean = row_sums[:, 0:1] * (1.0 / DC)
        square = row_sums[:, HD : HD + 1] * (1.0 / DC)
        scaled = (convd[rows, :] - mean) * lax.rsqrt(square - mean * mean + EPSILON) * cg_ref[...]
        result = (scaled * jax.nn.sigmoid(scaled)).astype(BF16)

        @pl.when(c == half)
        def _(result=result):
            conv_full[c] = result

        @pl.when(c != half)
        def _(result=result):
            conv_send[...] = result

    conv_copy = remote(conv_send, conv_full.at[c], cx_sem.at[0], cx_sem.at[1], partner)
    conv_copy.start()
    pending.append(conv_copy)

    for zs in range(NZ):

        @pl.when(jnp.logical_not((zs == z) & local))
        def _(zs=zs):
            remote(q_raw.at[zs], q_raw.at[zs], q_ss.at[0], q_rs.at[zs], partner).wait_recv()

        rows = q_raw[zs]
        zero = jnp.zeros_like(rows)
        low_half = low[:HALF]
        qs[zs, :HALF] = jnp.where(low_half, rows, zero)
        qs[zs, HALF:] = jnp.where(low_half, zero, rows)
    m_buf[...] = jnp.full_like(m_buf, NEG_FILL)
    acc[...] = jnp.zeros_like(acc)

    ones = jnp.ones((NX * 2 * HALF, 128), BF16)
    head_row = jnp.where(local, lam_ref[pl.ds(own_head, 1), :], lam_recv[pl.ds(own_head, 1), :])

    def tile(s, zt, diagonal):
        keys = kv_buf[s, :, 0:128]
        scores = lax.dot_general(
            qs[zt], keys, (((1,), (1,)), ((), ())), preferred_element_type=F32
        )
        if diagonal:
            row = lax.broadcasted_iota(jnp.int32, scores.shape, 0)
            col = lax.broadcasted_iota(jnp.int32, scores.shape, 1)
            query_segment = (x * 4 + c * 2) + ((row & (HALF - 1)) >> 6)
            scores = jnp.where((col >> 6) <= query_segment, scores, NEG_FILL)
        old = m_buf[zt]
        new = jnp.maximum(old, jnp.max(scores, axis=-1, keepdims=True))
        weights = jnp.exp(scores - jnp.concatenate([new] * 8, axis=1))
        factor = jnp.exp(old - new)
        rhs = jnp.concatenate([kv_buf[s, :, 128:256], ones], axis=1)
        part = jnp.dot(weights.astype(BF16), rhs, preferred_element_type=F32)
        acc[zt] = acc[zt] * jnp.concatenate([factor, factor], axis=1) + part
        m_buf[zt] = new

    def ret_copy(s):
        return remote(
            ret_send.at[s], attn_buf.at[z], ret_ss.at[s], ret_rs.at[z], {"sp": s * NX + x}
        )

    def log_copy(s):
        return remote(
            lsend.at[s], log_buf.at[own_head, c], log_ss.at[s], log_rs.at[own_head, c],
            {"sp": s * NX + x, "tp": src_tp},
        )

    def advance(s, carry):
        for relation, xs in enumerate((x, xl, xr, xo)):
            xs_o = xs
            ref = slot(s, xs_o, other)
            remote(ref, ref, d_ss.at[relation, s], d_rs.at[relation, s], partner).wait_recv()
        tile(s, s, True)
        pooled = acc[s]
        sums = pooled[:, 128:256]
        normal = pooled[:, 0:128] / sums
        head_out = normal[:HALF] - head_row * normal[HALF:]
        head_out = (
            head_out
            * lax.rsqrt(jnp.mean(head_out * head_out, axis=-1, keepdims=True) + EPSILON)
            * hg_ref[...]
            * HEAD_SCALE
        ).astype(BF16)
        logs = m_buf[s] + jnp.log(sums)
        first = jnp.transpose(logs[:HALF])[0:8]
        second = jnp.transpose(logs[HALF:])[0:8]
        sub = lax.broadcasted_iota(jnp.int32, (8, 128), 0)
        log_rows = jnp.where(sub == 0, first, second)
        ret_send[s] = head_out
        lsend[s] = log_rows

        @pl.when(s == z)
        def _():
            attn_buf[z] = head_out

        @pl.when((s == z) & local)
        def _():
            log_buf[own_head, c] = log_rows

        @pl.when(s != z)
        def _():
            ret_copy(s).start()

        @pl.when(jnp.logical_not((s == z) & local))
        def _():
            log_copy(s).start()

        def inner(zt, inner_carry):
            tile(s, zt, False)
            return inner_carry

        return lax.fori_loop(s + 1, NZ, inner, carry)

    lax.fori_loop(0, NZ, advance, 0)

    w_wait(1, 0)
    pending.append(w_share(yl, 1, 1))
    w_wait(0, 1)
    pending.append(w_share(yr, 0, 2))
    for kind in range(2):
        ref = w_buf.at[yo, c, kind]
        remote(ref, ref, w_ss.at[2, kind], w_rs.at[2, kind], up).wait_recv()
        pending.append(w_share(yo, kind, 3))
    conv_copy.wait_recv()
    for kind in range(2):
        for relation, source in enumerate((y, yl, yr, yo)):
            ref = w_buf.at[source, other, kind]
            remote(ref, ref, wd_ss.at[relation, kind], wd_rs.at[relation, kind], partner).wait_recv()

    for quarter in range(NY):
        cols = slice(quarter * 512, quarter * 512 + 512)
        acc_out[:, cols] = jnp.dot(
            conv_full[0], w_buf[quarter, 0, 0], preferred_element_type=F32
        ) + jnp.dot(conv_full[1], w_buf[quarter, 1, 0], preferred_element_type=F32)

    for hs in range(NZ):

        @pl.when(hs != z)
        def _(hs=hs):
            remote(
                attn_buf.at[hs], attn_buf.at[hs], ret_ss.at[hs], ret_rs.at[hs], partner
            ).wait_recv()

    sides = [jnp.concatenate([attn_buf[4 * side + k] for k in range(4)], axis=1) for side in range(2)]
    for quarter in range(NY):
        cols = slice(quarter * 512, quarter * 512 + 512)
        result = acc_out[:, cols]
        for side in range(2):
            result = result + jnp.dot(
                sides[side], w_buf[quarter, side, 1], preferred_element_type=F32
            )
        out_ref[:, cols] = result.astype(BF16)

    for head in range(4):
        for half in range(2):
            from_self = (4 * c + head == z) & (c == half)

            @pl.when(jnp.logical_not(from_self))
            def _(head=head, half=half):
                ref = log_buf.at[head, half]
                remote(ref, ref, log_ss.at[0], log_rs.at[head, half], partner).wait_recv()

            for which in range(2):
                log_ref[which, head : head + 1, half * HALF : half * HALF + HALF] = log_buf[
                    head, half, which : which + 1, :
                ]

    for away, kv_copy, q_copy in z_sends:

        @pl.when(away)
        def _(kv_copy=kv_copy, q_copy=q_copy):
            kv_copy.wait_send()
            q_copy.wait_send()

    for copy in pending:
        copy.wait_send()
    for s in range(NZ):

        @pl.when(s != z)
        def _(s=s):
            ret_copy(s).wait_send()

        @pl.when(jnp.logical_not((s == z) & local))
        def _(s=s):
            log_copy(s).wait_send()


def body(
    inputs,
    norm_gain,
    w_glu_value,
    w_glu_gate,
    w_query_one,
    w_query_two,
    w_key_one,
    w_key_two,
    w_value,
    conv_kernel,
    conv_gain,
    head_gain,
    lambda_head,
    w_out_conv,
    w_out_attn,
):
    lam = jnp.broadcast_to(jnp.pad(lambda_head, (0, 4))[:, None], (8, 128))
    vmem = pl.BlockSpec(memory_space=pltpu.VMEM)
    hbm = pl.BlockSpec(memory_space=pl.ANY)
    dma = pltpu.SemaphoreType.DMA
    mixed, logs = pl.pallas_call(
        kernel,
        out_shape=(
            jax.ShapeDtypeStruct((HALF, D), BF16),
            jax.ShapeDtypeStruct((2, 4, 2 * HALF), F32),
        ),
        in_specs=[vmem] * 6 + [hbm] * 9,
        out_specs=(vmem, vmem),
        scratch_shapes=[
            pltpu.VMEM((D, 512), BF16),
            pltpu.VMEM((D, 512), BF16),
            pltpu.VMEM((D, 256), BF16),
            pltpu.VMEM((D, 256), BF16),
            pltpu.VMEM((D, 256), BF16),
            pltpu.VMEM((D, 256), BF16),
            pltpu.VMEM((D, 512), BF16),
            pltpu.VMEM((2 * HALF, D), BF16),
            pltpu.VMEM((4, 2, HALF, 256), BF16),
            pltpu.VMEM((4, 2, HALF, 128), BF16),
            pltpu.VMEM((NZ, NX * 2 * HALF, 256), BF16),
            pltpu.VMEM((NZ, HALF, 128), BF16),
            pltpu.VMEM((NZ, 2 * HALF, 128), BF16),
            pltpu.VMEM((2 * HALF + 32, 512), F32),
            pltpu.VMEM((32, 512), BF16),
            pltpu.VMEM((32, 512), BF16),
            pltpu.VMEM((2 * HALF, 512), F32),
            pltpu.VMEM((2 * HALF, 128), F32),
            pltpu.VMEM((2 * HALF, 128), F32),
            pltpu.VMEM((2, HALF, 512), BF16),
            pltpu.VMEM((HALF, 512), BF16),
            pltpu.VMEM((NZ, 2 * HALF, 128), F32),
            pltpu.VMEM((NZ, 2 * HALF, 256), F32),
            pltpu.VMEM((NZ, HALF, 128), BF16),
            pltpu.VMEM((NZ, HALF, 128), BF16),
            pltpu.VMEM((NZ, 8, 128), F32),
            pltpu.VMEM((4, 2, 8, 128), F32),
            pltpu.VMEM((8, 128), F32),
            pltpu.VMEM((NY, 2, 2, 512, 512), BF16),
            pltpu.VMEM((HALF, D), F32),
            dma((7,)),
            dma((2,)),
            dma((8,)),
            dma((8,)),
            dma((NZ,)),
            dma((NZ,)),
            dma((4, NZ)),
            dma((4, NZ)),
            dma((4, NZ)),
            dma((4, NZ)),
            dma((2,)),
            dma((2,)),
            dma((2,)),
            dma((2,)),
            dma((NZ,)),
            dma((NZ,)),
            dma((NZ,)),
            dma((4, 2)),
            dma((3, 2)),
            dma((3, 2)),
            dma((4, 2)),
            dma((4, 2)),
            dma((2,)),
        ],
        compiler_params=pltpu.CompilerParams(
            collective_id=0, has_side_effects=True, vmem_limit_bytes=60 * 1024 * 1024
        ),
        name="mixer",
    )(
        inputs[0],
        norm_gain[None],
        conv_kernel.astype(F32),
        conv_gain[None],
        head_gain[None],
        lam,
        w_glu_value,
        w_glu_gate,
        w_query_one,
        w_query_two,
        w_key_one,
        w_key_two,
        w_value,
        w_out_conv,
        w_out_attn,
    )
    return (mixed[None], logs[None])


def solution(mesh):
    return jax.shard_map(
        body,
        mesh=mesh,
        in_specs=(
            P("fs", ("sp", "tp"), None),
            P(),
            P(None, "tp"),
            P(None, "tp"),
            P(None, "tp"),
            P(None, "tp"),
            P(None, "tp"),
            P(None, "tp"),
            P(None, "tp"),
            P(None, "tp"),
            P("tp"),
            P(),
            P("tp"),
            P("tp", "fs"),
            P("tp", "fs"),
        ),
        out_specs=(P("fs", ("sp", "tp"), None), P("fs", None, "tp", "sp")),
        check_vma=False,
    )
```

time: 524 us -> 106 us (0.20)
  matrix products: 151 us -> 0 us
  waiting for transfers between devices: 151 us -> 0 us
  local copies, waits for them, and re-layouts: 137 us -> 4.5 us
  Pallas kernels: 0 us -> 99.2 us
  other arithmetic: 39 us -> 1.39 us
  between operations: 14.1 us -> 0.64 us
  loops' own time: 11.2 us -> 0 us
  blocking collectives: 10.4 us -> 0 us
  starting transfers between devices: 6.79 us -> 0 us
    dot_general x73 -> x0, matrix products: 151 us -> none  [the longest x32 71.9 us: update(): jnp.einsum('tgrd,kgd->tgrk', queries, key_rows, preferred_element_type=jn...]
    all_gather x3 -> x0, waiting for transfers between devices: 149 us -> none  [the longest x1 138 us: body(): pieces = lax.all_gather(packed, 'sp', axis=0, tiled=True)]
    pallas_call x0 -> x1, Pallas kernels: none -> 99.2 us  [body(): pl.pallas_call(kernel, out_shape=(jax.ShapeDtypeStruct((HALF, D), BF16),...]
    reshape x3 -> x0, local copies, waits for them, and re-layouts: 38.4 us -> none  [the longest x1 13 us: body(): pieces[:, :key_local].reshape(block_count, block_rows, kv_local, HD)]
    dynamic_slice x48 -> x0, local copies, waits for them, and re-layouts: 34 us -> none  [body(): lax.scan(advance, running, (key_one_b, key_two_b, value_b, jnp.arange(blo...]
    unnamed x26 -> x2, local copies, waits for them, and re-layouts: 26.8 us -> 3.18 us
    while x320 -> x0, local copies, waits for them, and re-layouts: 23 us -> none
    reduce_sum x20 -> x0, other arithmetic: 21.9 us -> none  [the longest x16 16.5 us: update(): denominator = denominator * factor + jnp.sum(weights, axis=-1)]
  transfers between devices with their start and end apart: 5 -> 0, of which waited for: 3 -> 0; matrix products, arithmetic and copies ran while one was open for 57% -> 0% of each run, Pallas kernels for 0% -> 0%
where the time goes in v1:
time: 106 us
  Pallas kernels  99.2 us (94%)
  local copies, waits for them, and re-layouts  4.5 us (4%)
  other arithmetic  1.39 us (1%)
    pallas_call x1, Pallas kernels, body(): pl.pallas_call(kernel, out_shape=(jax.ShapeDtypeStruct((HALF, D), BF16),...  99.2 us
    unnamed x2, local copies, waits for them, and re-layouts  3.18 us

profile of v1, /device:TPU:1, one launch (start us, length us, event | category | flops | bytes accessed | tf_op | source)
XLA Modules:
  0.0 105.7 jit_solution(2162562071888833495)
XLA Ops:
  0.6 0.7 pad.4
  1.3 0.7 broadcast_in_dim.24.lam_ref
  2.0 1.4 %convert_element_type.5.ck_ref = f32[31,512]{1,0:T(8,128)} convert(bf16[31,512]{1,0:T(8,128)(2,1)} %param.24) | non-fusion elementwise | flops 15872 | bytes 95232 | tf_op jit(solution)/shard_map/convert_element_type | solution.py:653
  3.3 99.2 %mixer.1 = (bf16[128,2048]{1,0:T(8,128)(2,1)}, f32[2,4,256]{2,1,0:T(4,128)}) custom-call(bf16[128,2048]{1,0:T(8,128)(2,1)} %bitcast.6, f32[1,2048]{1,0:T(1,128)} %bitcast.9, f32[31,512]{1,0:T(8,128)} %convert_element_type.5.ck_ref, f32[1,512]{1,0:T(1,128)} %bitcast.10, f32[1,128]{1,0:T(1,128)} %bitcast.11, f32[8,128]{1,0:T(8,128)} %broadcast_in_dim.24.lam_ref, ...), custom_call_target="tpu_custom_call" | custom-call | tf_op jit(solution)/shard_map/mixer/pallas_call | solution.py:583
  102.6 1.9 %copy.19 = bf16[1,128,2048]{2,1,0:T(8,128)(2,1)} copy(bf16[1,128,2048]{2,1,0:T(8,128)(2,1)} %bitcast.7) | data formatting | bytes 1048576
  104.4 1.3 %copy.20 = f32[1,2,4,256]{3,2,1,0:T(4,128)} copy(f32[1,2,4,256]{3,2,1,0:T(4,128)} %bitcast.8) | data formatting | bytes 16384

commit v2 on v1

v2 whole, which is shorter than its diff:
```python
import jax
import jax.numpy as jnp
from jax import lax
from jax.experimental import pallas as pl
from jax.experimental.pallas import tpu as pltpu
from jax.sharding import PartitionSpec as P

D = 2048
DC = 1024
HD = 64
CW = 31
NZ = 8
NX = 4
NY = 4
HALF = 128
NEG_FILL = -1e30
EPSILON = 1e-05
HEAD_SCALE = 0.8
MESH = pl.DeviceIdType.MESH
F32 = jnp.float32
BF16 = jnp.bfloat16
W_ONE = 5
W_TWO = 8


def remote(src, dst, send_sem, recv_sem, device):
    return pltpu.make_async_remote_copy(
        src_ref=src,
        dst_ref=dst,
        send_sem=send_sem,
        recv_sem=recv_sem,
        device_id=device,
        device_id_type=MESH,
    )


def kernel(
    x_ref,
    gain_ref,
    ck_ref,
    cg_ref,
    hg_ref,
    lam_ref,
    wgv_hbm,
    wgg_hbm,
    wq1_hbm,
    wq2_hbm,
    wk1_hbm,
    wk2_hbm,
    wv_hbm,
    woc_hbm,
    woa_hbm,
    out_ref,
    log_ref,
    wgv,
    wgg,
    wq1,
    wq2,
    wk1,
    wk2,
    wv,
    normed,
    kv_send,
    q_send,
    kv_buf,
    q_raw,
    qs,
    gated_ext,
    halo_send,
    halo_recv,
    convd,
    sums_send,
    sums_recv,
    conv_full,
    conv_send,
    m_buf,
    acc,
    score_a,
    score_b,
    max_a,
    max_b,
    bias,
    gain_t,
    ret_send,
    attn_buf,
    lsend,
    log_buf,
    lam_own,
    lam_recv,
    w_buf,
    acc_out,
    load_sem,
    norm_sem,
    kv_ss,
    q_ss,
    kv_rs,
    q_rs,
    xs_ss,
    xs_rs,
    d_ss,
    d_rs,
    halo_sem,
    sums_sem,
    cx_sem,
    lam_sem,
    ret_ss,
    ret_rs,
    log_ss,
    log_rs,
    w_ss,
    w_rs,
    wx_ss,
    wx_rs,
    wd_ss,
    wd_rs,
    wp_ss,
    wp_rs,
    own_sem,
):
    me = lax.axis_index("sp")
    y = lax.axis_index("fs")
    c = lax.axis_index("tp")
    z, x = me // NX, me % NX
    other = 1 - c
    xr, xl, xo = (x + 1) % NX, (x + 3) % NX, (x + 2) % NX
    yr, yl, yo = (y + 1) % NY, (y + 3) % NY, (y + 2) % NY
    src_tp = z // 4
    own_head = z % 4
    local = src_tp == c
    partner = {"tp": other}
    right = {"sp": z * NX + xr}
    left = {"sp": z * NX + xl}
    up = {"fs": yr}
    down = {"fs": yl}
    following = {"sp": (me + 1) % (NZ * NX)}
    preceding = {"sp": (me + NZ * NX - 1) % (NZ * NX)}
    pending = []

    def begin(copy):
        copy.start()
        pending.append(copy)
        return copy

    loads = []
    for index, (src, dst) in enumerate(
        ((wv_hbm, wv), (wk1_hbm, wk1), (wk2_hbm, wk2), (wq1_hbm, wq1), (wq2_hbm, wq2),
         (wgv_hbm, wgv), (wgg_hbm, wgg))
    ):
        loads.append(pltpu.make_async_copy(src, dst, load_sem.at[index]))
        loads[-1].start()

    barrier = pltpu.get_barrier_semaphore()
    for device in (partner, right, left, up, down, following, preceding):
        pl.semaphore_signal(barrier, inc=1, device_id=device, device_id_type=MESH)
    for step in range(1, NZ):
        for core in range(2):
            pl.semaphore_signal(
                barrier,
                inc=1,
                device_id={"sp": ((z + step) % NZ) * NX + x, "tp": core},
                device_id_type=MESH,
            )

    my_rows = pl.multiple_of(c * HALF, HALF)
    peer_rows = pl.multiple_of(other * HALF, HALF)
    for part in range(4):
        rows_f = x_ref[part * 32 : part * 32 + 32, :].astype(F32)
        scale = lax.rsqrt(jnp.mean(rows_f * rows_f, axis=-1, keepdims=True) + EPSILON)
        normed[pl.ds(my_rows + part * 32, 32), :] = (rows_f * scale * gain_ref[...]).astype(BF16)

    lane = lax.broadcasted_iota(jnp.int32, (HALF, 128), 1)
    low = lane < HD

    def head_pair(one, two, head):
        pair = slice((head // 2) * 128, (head // 2) * 128 + 128)
        first, second = one[:, pair], two[:, pair]
        if head % 2 == 0:
            return jnp.where(low, first, pltpu.roll(second, HD, 1))
        return jnp.where(low, pltpu.roll(first, HD, 1), second)

    def project_qkv(rows, half, fresh):
        block = normed[pl.ds(rows, HALF), :]

        def project(index, weight):
            if fresh:
                loads[index].wait()
            return jnp.dot(block, weight[...], preferred_element_type=F32)

        values = project(0, wv)
        for head in range(4):
            kv_send[head, half, :, 128:256] = jnp.transpose(
                values[:, head * 128 : head * 128 + 128]
            ).astype(BF16)
        key_one = project(1, wk1)
        key_two = project(2, wk2)
        for head in range(4):
            kv_send[head, half, :, 0:128] = head_pair(key_one, key_two, head).astype(BF16)
        query_one = project(3, wq1)
        query_two = project(4, wq2)
        for head in range(4):
            q_send[head, half] = (head_pair(query_one, query_two, head) * (HD**-0.5)).astype(BF16)

    def project_glu(rows, fresh):
        block = normed[pl.ds(rows, HALF), :]
        if fresh:
            loads[5].wait()
            loads[6].wait()
        value = jnp.dot(block, wgv[...], preferred_element_type=F32).astype(BF16).astype(F32)
        gate = jnp.dot(block, wgg[...], preferred_element_type=F32).astype(BF16).astype(F32)
        gated = (value * jax.nn.sigmoid(gate)).astype(BF16)
        gated_ext[pl.ds(pl.multiple_of(rows + 32, 32), HALF), :] = gated.astype(F32)

    project_qkv(my_rows, c, True)
    for index in range(4):
        lam_own[index : index + 1, :] = jnp.full((1, 128), lam_ref[index], F32)
    lam_own[4:8, :] = jnp.zeros((4, 128), F32)

    pl.semaphore_wait(barrier, 7 + 2 * (NZ - 1))

    mine = normed.at[pl.ds(my_rows, HALF), :]
    norm_copy = begin(remote(mine, mine, norm_sem.at[0], norm_sem.at[1], partner))

    def slot(zs, xs, cs):
        return kv_buf.at[zs, pl.ds(pl.multiple_of((xs * 2 + cs) * HALF, HALF), HALF), :]

    def slot_half(zs, xs, cs, part):
        start = pl.multiple_of((xs * 2 + cs) * HALF + part * (HALF // 2), HALF // 2)
        return kv_buf.at[zs, pl.ds(start, HALF // 2), :]

    u = z % 4
    ranks = (u, u + 1 - 2 * (u % 2), 2 - u // 2, 3 * (1 - u // 2))
    same = 1 - src_tp - c + 2 * src_tp * c
    z_sends = []

    def z_send(rank, half, index):
        head = same * ranks[rank] + (1 - same) * ranks[3 - rank]
        target = 4 * c + head
        device = {"sp": target * NX + x, "tp": half}
        kv_copy = remote(
            kv_send.at[head, half], slot(z, x, half), kv_ss.at[index], kv_rs.at[z], device
        )
        q_copy = remote(q_send.at[head, half], q_raw.at[z], q_ss.at[index], q_rs.at[z], device)
        away = jnp.logical_not((target == z) & (half == c))
        z_sends.append((away, kv_copy, q_copy))

        @pl.when(away)
        def _():
            kv_copy.start()
            q_copy.start()

    z_send(0, c, 0)
    z_send(1, c, 1)

    @pl.when(local)
    def _():
        kv_buf[z, pl.ds(pl.multiple_of((x * 2 + c) * HALF, HALF), HALF), :] = kv_send[own_head, c]
        q_raw[z] = q_send[own_head, c]

    w_hbm = (woc_hbm, woa_hbm)

    def w_own(side, kind, device):
        begin(remote(w_hbm[kind], w_buf.at[y, c, kind], w_ss.at[side, kind], w_rs.at[side, kind], device))

    w_own(0, 0, up)
    w_own(1, 1, down)
    lam_copy = begin(remote(lam_own, lam_recv, lam_sem.at[0], lam_sem.at[1], partner))

    project_glu(my_rows, True)
    norm_copy.wait_recv()
    project_qkv(peer_rows, other, False)
    z_send(0, other, 2)
    z_send(1, other, 3)
    z_send(2, c, 4)
    z_send(2, other, 5)
    z_send(3, c, 6)
    z_send(3, other, 7)
    project_glu(peer_rows, False)
    halo_send[...] = gated_ext[2 * HALF :, :].astype(BF16)
    halo_copy = begin(remote(halo_send, halo_recv, halo_sem.at[0], halo_sem.at[1], following))

    own_w = []
    for kind in range(2):
        own = pltpu.make_async_copy(w_hbm[kind], w_buf.at[y, c, kind], own_sem.at[kind])
        own.start()
        own_w.append(own)
        begin(remote(w_hbm[kind], w_buf.at[y, c, kind], wd_ss.at[0, kind], wd_rs.at[0, kind], partner))

    taps = ck_ref[...].astype(F32)

    def conv_chunk(part):
        base = part * 32
        total = None
        for shift in range(8):
            partial = None
            span = 32 if shift == 0 else 40
            for group in range(5):
                tap = 8 * group + shift - 2
                if tap < 0 or tap >= CW:
                    continue
                term = taps[tap : tap + 1, :] * gated_ext[base + 8 * group : base + 8 * group + span, :]
                partial = term if partial is None else partial + term
            moved = partial[shift : shift + 32, :]
            total = moved if total is None else total + moved
        convd[base : base + 32, :] = total
        sums = jnp.sum(total, axis=-1, keepdims=True)
        squares = jnp.sum(total * total, axis=-1, keepdims=True)
        sums_send[base : base + 32, :] = jnp.where(low[:32], sums, squares)

    def stage_one(zs):
        ref = slot(zs, x, c)
        away = jnp.logical_not((zs == z) & local)

        @pl.when(away)
        def _():
            remote(ref, ref, kv_ss.at[0], kv_rs.at[zs], partner).wait_recv()

        begin(remote(ref, ref, xs_ss.at[0, zs], xs_rs.at[0, zs], right))
        begin(remote(ref, ref, xs_ss.at[1, zs], xs_rs.at[1, zs], left))
        begin(remote(ref, ref, d_ss.at[0, zs], d_rs.at[0, zs], partner))

        @pl.when(away)
        def _():
            remote(q_raw.at[zs], q_raw.at[zs], q_ss.at[0], q_rs.at[zs], partner).wait_recv()

        rows = q_raw[zs]
        zero = jnp.zeros_like(rows)
        qs[zs, :HALF] = jnp.where(low, rows, zero)
        qs[zs, HALF:] = jnp.where(low, zero, rows)

    def stage_two(zs):
        ref = slot(zs, xl, c)
        remote(ref, ref, xs_ss.at[0, zs], xs_rs.at[0, zs], right).wait_recv()
        part = slot_half(zs, xl, c, 0)
        begin(remote(part, part, xs_ss.at[2, zs], xs_rs.at[2, zs], right))
        begin(remote(ref, ref, d_ss.at[1, zs], d_rs.at[1, zs], partner))
        ref = slot(zs, xr, c)
        remote(ref, ref, xs_ss.at[1, zs], xs_rs.at[1, zs], left).wait_recv()
        part = slot_half(zs, xr, c, 1)
        begin(remote(part, part, xs_ss.at[3, zs], xs_rs.at[3, zs], left))
        begin(remote(ref, ref, d_ss.at[2, zs], d_rs.at[2, zs], partner))

    def stage_three(zs):
        for part in range(2):
            ref = slot_half(zs, xo, c, part)
            remote(ref, ref, xs_ss.at[2 + part, zs], xs_rs.at[2 + part, zs], right).wait_recv()
        ref = slot(zs, xo, c)
        begin(remote(ref, ref, d_ss.at[3, zs], d_rs.at[3, zs], partner))

    def stage_four(zs):
        for relation, xs in enumerate((x, xl, xr, xo)):
            ref = slot(zs, xs, other)
            remote(ref, ref, d_ss.at[relation, zs], d_rs.at[relation, zs], partner).wait_recv()

    def w_wait(source, kind, side):
        ref = w_buf.at[source, c, kind]
        remote(ref, ref, w_ss.at[side, kind], w_rs.at[side, kind], up).wait_recv()

    def w_share(source, kind, relation):
        ref = w_buf.at[source, c, kind]
        begin(remote(ref, ref, wd_ss.at[relation, kind], wd_rs.at[relation, kind], partner))

    def piece(source, core, kind, xs):
        return w_buf.at[source, core, kind, pl.ds(pl.multiple_of(xs * 128, 128), 128), :]

    def piece_share(kind, relation, xs):
        ref = piece(yo, c, kind, xs)
        begin(remote(ref, ref, wp_ss.at[relation, kind], wp_rs.at[relation, kind], partner))

    def w_one():
        w_wait(yl, 0, 0)
        ref = piece(yl, c, 0, x)
        begin(remote(ref, ref, w_ss.at[2, 0], w_rs.at[2, 0], up))
        w_own(0, 1, up)
        w_wait(yr, 1, 1)
        ref = piece(yr, c, 1, x)
        begin(remote(ref, ref, w_ss.at[2, 1], w_rs.at[2, 1], down))
        w_own(1, 0, down)
        w_share(yl, 0, 1)
        w_share(yr, 1, 2)

    def w_two():
        for kind in range(2):
            ref = piece(yo, c, kind, x)
            remote(ref, ref, w_ss.at[2, kind], w_rs.at[2, kind], up).wait_recv()
            begin(remote(ref, ref, wx_ss.at[0, kind], wx_rs.at[0, kind], right))
            begin(remote(ref, ref, wx_ss.at[1, kind], wx_rs.at[1, kind], left))
            piece_share(kind, 0, x)

    def w_three():
        for kind in range(2):
            for side, xs in ((0, xl), (1, xr)):
                ref = piece(yo, c, kind, xs)
                remote(ref, ref, wx_ss.at[side, kind], wx_rs.at[side, kind], right).wait_recv()
                if side == kind:
                    device = right if side == 0 else left
                    begin(remote(ref, ref, wx_ss.at[2, kind], wx_rs.at[2, kind], device))
                piece_share(kind, 1 + side, xs)

    def w_four():
        w_wait(yl, 1, 0)
        w_share(yl, 1, 1)
        w_wait(yr, 0, 1)
        w_share(yr, 0, 2)
        for kind in range(2):
            ref = piece(yo, c, kind, xo)
            remote(ref, ref, wx_ss.at[2, kind], wx_rs.at[2, kind], right).wait_recv()
            piece_share(kind, 3, xo)

    def w_five(kind):
        for relation, source in enumerate((y, yl, yr)):
            ref = w_buf.at[source, other, kind]
            remote(ref, ref, wd_ss.at[relation, kind], wd_rs.at[relation, kind], partner).wait_recv()
        for relation, xs in enumerate((x, xl, xr, xo)):
            ref = piece(yo, other, kind, xs)
            remote(ref, ref, wp_ss.at[relation, kind], wp_rs.at[relation, kind], partner).wait_recv()

    def conv_finish():
        sums_copy.wait_recv()
        for half in range(2):
            rows = slice(half * HALF, half * HALF + HALF)
            row_sums = sums_send[rows, :] + sums_recv[rows, :]
            mean = row_sums[:, 0:1] * (1.0 / DC)
            square = row_sums[:, HD : HD + 1] * (1.0 / DC)
            scaled = (convd[rows, :] - mean) * lax.rsqrt(square - mean * mean + EPSILON) * cg_ref[...]
            result = (scaled * jax.nn.sigmoid(scaled)).astype(BF16)

            @pl.when(c == half)
            def _(result=result):
                conv_full[c] = result

            @pl.when(c != half)
            def _(result=result):
                conv_send[...] = result

        return begin(remote(conv_send, conv_full.at[c], cx_sem.at[0], cx_sem.at[1], partner))

    m_buf[...] = jnp.full_like(m_buf, NEG_FILL)
    acc[...] = jnp.zeros_like(acc)
    bias[0] = jnp.zeros((16, 8, 256), F32)
    query_segment = (x * 4 + c * 2) + (
        (lax.broadcasted_iota(jnp.int32, (8, 256), 1) & (HALF - 1)) >> 6
    )
    for segment in range(16):
        bias[1, segment] = jnp.where(query_segment >= segment, 0.0, NEG_FILL)
    gain_t[...] = jnp.transpose(jnp.broadcast_to(hg_ref[...], (128, 128))) * HEAD_SCALE

    def place(index):
        odd = index % 2
        offset = odd * ((index + 1) // 2) + (1 - odd) * (NZ - index // 2)
        return (z + offset) % NZ

    def which(t):
        i = 0
        for bound in (1, 3, 6, 10, 15, 21, 28):
            i = i + jnp.where(t >= bound, 1, 0)
        j = t - (i * (i + 1)) // 2
        zi, zj = place(i), place(j)
        return jnp.minimum(zi, zj), jnp.maximum(zi, zj), (j + 1) // (i + 1)

    def scores(t, score_ref, max_ref):
        s, zt, kind = which(t)
        queries = qs[zt]
        best = None
        for start in range(0, 1024, 256):
            block = lax.dot_general(
                kv_buf[s, start : start + 256, 0:128],
                queries,
                (((1,), (1,)), ((), ())),
                preferred_element_type=F32,
            )
            score_ref[start : start + 256] = block
            for inner in range(4):
                top = None
                for row in range(inner * 64, inner * 64 + 64, 8):
                    top = block[row : row + 8] if top is None else jnp.maximum(top, block[row : row + 8])
                top = top + bias[kind, start // 64 + inner]
                best = top if best is None else jnp.maximum(best, top)
        max_ref[...] = best

    ones = jnp.ones((16, 256), BF16)

    def absorb(t, score_ref, max_ref):
        s, zt, kind = which(t)
        old = m_buf[zt, 0:1]
        new = jnp.maximum(old, jnp.max(max_ref[...], axis=0, keepdims=True))
        factor = jnp.exp(old - new)
        total = None
        for start in range(0, 1024, 256):
            weights = []
            for inner in range(4):
                row = start + inner * 64
                shifted = new - bias[kind, row // 64, 0:1]
                weights.append(jnp.exp(score_ref[row : row + 64] - shifted).astype(BF16))
            lhs = jnp.concatenate(
                [
                    jnp.concatenate(
                        [
                            kv_buf[s, start : start + 128, 128:256],
                            kv_buf[s, start + 128 : start + 256, 128:256],
                        ],
                        axis=1,
                    ),
                    ones,
                ],
                axis=0,
            )
            part = jnp.dot(lhs, jnp.concatenate(weights, axis=0), preferred_element_type=F32)
            total = part if total is None else total + part
        acc[zt] = acc[zt] * factor + total
        m_buf[zt] = jnp.broadcast_to(new, (8, 256))

    def ret_copy(s):
        return remote(
            ret_send.at[s], attn_buf.at[z], ret_ss.at[s], ret_rs.at[z], {"sp": s * NX + x}
        )

    def log_copy(s):
        return remote(
            lsend.at[s], log_buf.at[own_head, c], log_ss.at[s], log_rs.at[own_head, c],
            {"sp": s * NX + x, "tp": src_tp},
        )

    def finish(s):
        sums = acc[s, 128:129, :]
        normal = acc[s, 0:128, :] * (1.0 / sums)
        lam_row = jnp.where(local, lam_own[pl.ds(own_head, 1), :], lam_recv[pl.ds(own_head, 1), :])
        head_out = normal[:, :HALF] - lam_row * normal[:, HALF:]
        head_out = (
            head_out
            * lax.rsqrt(jnp.mean(head_out * head_out, axis=0, keepdims=True) + EPSILON)
            * gain_t[...]
        )
        head_out = jnp.transpose(head_out).astype(BF16)
        logs = m_buf[s, 0:1] + jnp.log(sums)
        sub = lax.broadcasted_iota(jnp.int32, (8, 128), 0)
        log_rows = jnp.where(sub == 0, logs[:, :HALF], logs[:, HALF:])
        ret_send[s] = head_out
        lsend[s] = log_rows

        @pl.when(s == z)
        def _():
            attn_buf[z] = head_out

        @pl.when((s == z) & local)
        def _():
            log_buf[own_head, c] = log_rows

        @pl.when(s != z)
        def _():
            ret_copy(s).start()

        @pl.when(jnp.logical_not((s == z) & local))
        def _():
            log_copy(s).start()

    def pair(p, carry):
        scores(2 * p + 1, score_b, max_b)
        absorb(2 * p, score_a, max_a)
        scores(2 * p + 2, score_a, max_a)
        absorb(2 * p + 1, score_b, max_b)
        return carry

    last = place(NZ - 1)
    conv_copy = None
    done_pairs = 0
    for step in range(NZ + 2):
        if step < NZ:
            stage_one(place(step))
        if step == 0:
            for part in (1, 2, 3, 4, 5, 6, 7):
                conv_chunk(part)
            halo_copy.wait_recv()
            rows = halo_recv[...].astype(F32)
            gated_ext[0:32, :] = jnp.where(me == 0, jnp.zeros_like(rows), rows)
            conv_chunk(0)
            sums_copy = begin(remote(sums_send, sums_recv, sums_sem.at[0], sums_sem.at[1], partner))
        if 0 <= step - 1 < NZ:
            stage_two(place(step - 1))
        if step == 2:
            conv_copy = conv_finish()
        if step == NZ + 1:
            lam_copy.wait_recv()

            def early(j, carry):
                zj = place(j)

                @pl.when(zj < last)
                def _():
                    finish(zj)

                return carry

            lax.fori_loop(0, 5, early, 0)
        if 0 <= step - 2 < NZ:
            stage_three(place(step - 2))
        if step == W_ONE:
            w_one()
        if step == W_TWO:
            w_two()
        if 0 <= step - 2 < NZ:
            index = step - 2
            stage_four(place(index))
            if index == 0:
                scores(0, score_a, max_a)
            else:
                end = ((index + 1) * (index + 2) // 2 - 1) // 2
                lax.fori_loop(done_pairs, end, pair, 0)
                done_pairs = end
    scores(35, score_b, max_b)
    absorb(34, score_a, max_a)
    absorb(35, score_b, max_b)

    def late(j, carry):
        zj = place(j)

        @pl.when((j > 4) | (zj > last))
        def _():
            finish(zj)

        return carry

    lax.fori_loop(0, NZ, late, 0)

    w_three()
    w_four()
    for kind in range(2):
        own_w[kind].wait()
    conv_copy.wait_recv()
    w_five(0)
    for quarter in range(NY):
        cols = slice(quarter * 512, quarter * 512 + 512)
        acc_out[:, cols] = jnp.dot(
            conv_full[0], w_buf[quarter, 0, 0], preferred_element_type=F32
        ) + jnp.dot(conv_full[1], w_buf[quarter, 1, 0], preferred_element_type=F32)
    w_five(1)

    for hs in range(NZ):

        @pl.when(hs != z)
        def _(hs=hs):
            remote(
                attn_buf.at[hs], attn_buf.at[hs], ret_ss.at[hs], ret_rs.at[hs], partner
            ).wait_recv()

    sides = [jnp.concatenate([attn_buf[4 * side + k] for k in range(4)], axis=1) for side in range(2)]
    for quarter in range(NY):
        cols = slice(quarter * 512, quarter * 512 + 512)
        result = acc_out[:, cols]
        for side in range(2):
            result = result + jnp.dot(
                sides[side], w_buf[quarter, side, 1], preferred_element_type=F32
            )
        out_ref[:, cols] = result.astype(BF16)

    for head in range(4):
        for half in range(2):
            from_self = (4 * c + head == z) & (c == half)

            @pl.when(jnp.logical_not(from_self))
            def _(head=head, half=half):
                ref = log_buf.at[head, half]
                remote(ref, ref, log_ss.at[0], log_rs.at[head, half], partner).wait_recv()

            for which_map in range(2):
                log_ref[which_map, head : head + 1, half * HALF : half * HALF + HALF] = log_buf[
                    head, half, which_map : which_map + 1, :
                ]

    for away, kv_copy, q_copy in z_sends:

        @pl.when(away)
        def _(kv_copy=kv_copy, q_copy=q_copy):
            kv_copy.wait_send()
            q_copy.wait_send()

    for copy in pending:
        copy.wait_send()
    for s in range(NZ):

        @pl.when(s != z)
        def _(s=s):
            ret_copy(s).wait_send()

        @pl.when(jnp.logical_not((s == z) & local))
        def _(s=s):
            log_copy(s).wait_send()


def body(
    inputs,
    norm_gain,
    w_glu_value,
    w_glu_gate,
    w_query_one,
    w_query_two,
    w_key_one,
    w_key_two,
    w_value,
    conv_kernel,
    conv_gain,
    head_gain,
    lambda_head,
    w_out_conv,
    w_out_attn,
):
    vmem = pl.BlockSpec(memory_space=pltpu.VMEM)
    hbm = pl.BlockSpec(memory_space=pl.ANY)
    dma = pltpu.SemaphoreType.DMA
    mixed, logs = pl.pallas_call(
        kernel,
        out_shape=(
            jax.ShapeDtypeStruct((HALF, D), BF16),
            jax.ShapeDtypeStruct((2, 4, 2 * HALF), F32),
        ),
        in_specs=[vmem] * 5 + [pl.BlockSpec(memory_space=pltpu.SMEM)] + [hbm] * 9,
        out_specs=(vmem, vmem),
        scratch_shapes=[
            pltpu.VMEM((D, 512), BF16),
            pltpu.VMEM((D, 512), BF16),
            pltpu.VMEM((D, 256), BF16),
            pltpu.VMEM((D, 256), BF16),
            pltpu.VMEM((D, 256), BF16),
            pltpu.VMEM((D, 256), BF16),
            pltpu.VMEM((D, 512), BF16),
            pltpu.VMEM((2 * HALF, D), BF16),
            pltpu.VMEM((4, 2, HALF, 256), BF16),
            pltpu.VMEM((4, 2, HALF, 128), BF16),
            pltpu.VMEM((NZ, NX * 2 * HALF, 256), BF16),
            pltpu.VMEM((NZ, HALF, 128), BF16),
            pltpu.VMEM((NZ, 2 * HALF, 128), BF16),
            pltpu.VMEM((2 * HALF + 32, 512), F32),
            pltpu.VMEM((32, 512), BF16),
            pltpu.VMEM((32, 512), BF16),
            pltpu.VMEM((2 * HALF, 512), F32),
            pltpu.VMEM((2 * HALF, 128), F32),
            pltpu.VMEM((2 * HALF, 128), F32),
            pltpu.VMEM((2, HALF, 512), BF16),
            pltpu.VMEM((HALF, 512), BF16),
            pltpu.VMEM((NZ, 8, 256), F32),
            pltpu.VMEM((NZ, 144, 256), F32),
            pltpu.VMEM((1024, 256), F32),
            pltpu.VMEM((1024, 256), F32),
            pltpu.VMEM((8, 256), F32),
            pltpu.VMEM((8, 256), F32),
            pltpu.VMEM((2, 16, 8, 256), F32),
            pltpu.VMEM((128, 128), F32),
            pltpu.VMEM((NZ, HALF, 128), BF16),
            pltpu.VMEM((NZ, HALF, 128), BF16),
            pltpu.VMEM((NZ, 8, 128), F32),
            pltpu.VMEM((4, 2, 8, 128), F32),
            pltpu.VMEM((8, 128), F32),
            pltpu.VMEM((8, 128), F32),
            pltpu.VMEM((NY, 2, 2, 512, 512), BF16),
            pltpu.VMEM((HALF, D), F32),
            dma((7,)),
            dma((2,)),
            dma((8,)),
            dma((8,)),
            dma((NZ,)),
            dma((NZ,)),
            dma((4, NZ)),
            dma((4, NZ)),
            dma((4, NZ)),
            dma((4, NZ)),
            dma((2,)),
            dma((2,)),
            dma((2,)),
            dma((2,)),
            dma((NZ,)),
            dma((NZ,)),
            dma((NZ,)),
            dma((4, 2)),
            dma((3, 2)),
            dma((3, 2)),
            dma((3, 2)),
            dma((3, 2)),
            dma((3, 2)),
            dma((3, 2)),
            dma((4, 2)),
            dma((4, 2)),
            dma((2,)),
        ],
        compiler_params=pltpu.CompilerParams(
            collective_id=0, has_side_effects=True, vmem_limit_bytes=60 * 1024 * 1024
        ),
        name="mixer",
    )(
        inputs[0],
        norm_gain[None],
        conv_kernel,
        conv_gain[None],
        head_gain[None],
        lambda_head,
        w_glu_value,
        w_glu_gate,
        w_query_one,
        w_query_two,
        w_key_one,
        w_key_two,
        w_value,
        w_out_conv,
        w_out_attn,
    )
    return (mixed[None], logs[None])


def solution(mesh):
    return jax.shard_map(
        body,
        mesh=mesh,
        in_specs=(
            P("fs", ("sp", "tp"), None),
            P(),
            P(None, "tp"),
            P(None, "tp"),
            P(None, "tp"),
            P(None, "tp"),
            P(None, "tp"),
            P(None, "tp"),
            P(None, "tp"),
            P(None, "tp"),
            P("tp"),
            P(),
            P("tp"),
            P("tp", "fs"),
            P("tp", "fs"),
        ),
        out_specs=(P("fs", ("sp", "tp"), None), P("fs", None, "tp", "sp")),
        check_vma=False,
    )
```

time: 106 us -> 81.4 us (0.77)
  Pallas kernels: 99.2 us -> 77.4 us
  other arithmetic: 1.39 us -> 0 us
  local copies, waits for them, and re-layouts: 4.5 us -> 3.18 us
    pallas_call x1, Pallas kernels: 99.2 us -> 77.4 us  [body(): pl.pallas_call(kernel, out_shape=(jax.ShapeDtypeStruct((HALF, D), BF16),...]
    convert_element_type x1 -> x0, other arithmetic: 1.39 us -> none  [body(): conv_kernel.astype(F32)]
where the time goes in v2:
time: 81.4 us; the launch traced here: 81.2 us
  Pallas kernels  77.4 us (95%)
  local copies, waits for them, and re-layouts  3.18 us (4%)
    pallas_call x1, Pallas kernels, body(): pl.pallas_call(kernel, out_shape=(jax.ShapeDtypeStruct((HALF, D), BF16),...  77.4 us
    unnamed x2, local copies, waits for them, and re-layouts  3.18 us

profile of v2, /device:TPU:1, one launch (start us, length us, event | category | flops | bytes accessed | tf_op | source)
XLA Modules:
  0.0 81.2 jit_solution(11371951636719834967)
XLA Ops:
  0.6 77.4 %mixer.1 = (bf16[128,2048]{1,0:T(8,128)(2,1)}, f32[2,4,256]{2,1,0:T(4,128)}) custom-call(bf16[128,2048]{1,0:T(8,128)(2,1)} %bitcast.6, f32[1,2048]{1,0:T(1,128)} %bitcast.8, bf16[31,512]{1,0:T(8,128)(2,1)} %ck_ref.1, f32[1,512]{1,0:T(1,128)} %bitcast.10, f32[1,128]{1,0:T(1,128)} %bitcast.11, f32[4]{0:T(128)} %lam_ref.1, bf16[2048,512]{1,0:T(8,128)(2,1)} %wgv_hbm.1, ...), custom_call_target="tpu_custom_call" | custom-call | tf_op jit(solution)/shard_map/mixer/pallas_call | solution.py:709
  78.0 1.9 %copy.19 = bf16[1,128,2048]{2,1,0:T(8,128)(2,1)} copy(bf16[1,128,2048]{2,1,0:T(8,128)(2,1)} %bitcast.7) | data formatting | bytes 1048576
  79.9 1.3 %copy.20 = f32[1,2,4,256]{3,2,1,0:T(4,128)} copy(f32[1,2,4,256]{3,2,1,0:T(4,128)} %bitcast.9) | data formatting | bytes 16384

commit v3 on v2

--- a/solution.py
+++ b/solution.py
@@ -13,14 +13,15 @@
 NX = 4
 NY = 4
 HALF = 128
+Z_GATE = 2
+V_SPLIT = 5
+W_THREE = 5
 NEG_FILL = -1e30
 EPSILON = 1e-05
 HEAD_SCALE = 0.8
 MESH = pl.DeviceIdType.MESH
 F32 = jnp.float32
 BF16 = jnp.bfloat16
-W_ONE = 5
-W_TWO = 8
 
 
 def remote(src, dst, send_sem, recv_sem, device):
@@ -60,9 +61,11 @@
     wk2,
     wv,
     normed,
-    kv_send,
+    k_send,
+    v_send,
     q_send,
-    kv_buf,
+    k_buf,
+    v_buf,
     q_raw,
     qs,
     gated_ext,
@@ -91,10 +94,8 @@
     acc_out,
     load_sem,
     norm_sem,
-    kv_ss,
-    q_ss,
-    kv_rs,
-    q_rs,
+    z_ss,
+    z_rs,
     xs_ss,
     xs_rs,
     d_ss,
@@ -143,11 +144,12 @@
 
     loads = []
     for index, (src, dst) in enumerate(
-        ((wv_hbm, wv), (wk1_hbm, wk1), (wk2_hbm, wk2), (wq1_hbm, wq1), (wq2_hbm, wq2),
+        ((wk1_hbm, wk1), (wk2_hbm, wk2), (wv_hbm, wv), (wq1_hbm, wq1), (wq2_hbm, wq2),
          (wgv_hbm, wgv), (wgg_hbm, wgg))
     ):
         loads.append(pltpu.make_async_copy(src, dst, load_sem.at[index]))
-        loads[-1].start()
+        if index < 2:
+            loads[-1].start()
 
     barrier = pltpu.get_barrier_semaphore()
     for device in (partner, right, left, up, down, following, preceding):
@@ -178,27 +180,27 @@
             return jnp.where(low, first, pltpu.roll(second, HD, 1))
         return jnp.where(low, pltpu.roll(first, HD, 1), second)
 
-    def project_qkv(rows, half, fresh):
-        block = normed[pl.ds(rows, HALF), :]
-
-        def project(index, weight):
-            if fresh:
-                loads[index].wait()
-            return jnp.dot(block, weight[...], preferred_element_type=F32)
-
-        values = project(0, wv)
+    def project(rows, index, weight, fresh):
+        if fresh:
+            loads[index].wait()
+        return jnp.dot(normed[pl.ds(rows, HALF), :], weight[...], preferred_element_type=F32)
+
+    def project_keys(rows, half, fresh):
+        one = project(rows, 0, wk1, fresh)
+        two = project(rows, 1, wk2, fresh)
         for head in range(4):
-            kv_send[head, half, :, 128:256] = jnp.transpose(
-                values[:, head * 128 : head * 128 + 128]
-            ).astype(BF16)
-        key_one = project(1, wk1)
-        key_two = project(2, wk2)
+            k_send[head, half] = head_pair(one, two, head).astype(BF16)
+
+    def project_values(rows, half, fresh):
+        values = project(rows, 2, wv, fresh)
         for head in range(4):
-            kv_send[head, half, :, 0:128] = head_pair(key_one, key_two, head).astype(BF16)
-        query_one = project(3, wq1)
-        query_two = project(4, wq2)
+            v_send[head, half] = jnp.transpose(values[:, head * 128 : head * 128 + 128]).astype(BF16)
+
+    def project_queries(rows, half, fresh):
+        one = project(rows, 3, wq1, fresh)
+        two = project(rows, 4, wq2, fresh)
         for head in range(4):
-            q_send[head, half] = (head_pair(query_one, query_two, head) * (HD**-0.5)).astype(BF16)
+            q_send[head, half] = (head_pair(one, two, head) * (HD**-0.5)).astype(BF16)
 
     def project_glu(rows, fresh):
         block = normed[pl.ds(rows, HALF), :]
@@ -210,7 +212,9 @@
         gated = (value * jax.nn.sigmoid(gate)).astype(BF16)
         gated_ext[pl.ds(pl.multiple_of(rows + 32, 32), HALF), :] = gated.astype(F32)
 
-    project_qkv(my_rows, c, True)
+    project_keys(my_rows, c, True)
+    for load in loads[2:]:
+        load.start()
     for index in range(4):
         lam_own[index : index + 1, :] = jnp.full((1, 128), lam_ref[index], F32)
     lam_own[4:8, :] = jnp.zeros((4, 128), F32)
@@ -220,41 +224,49 @@
     mine = normed.at[pl.ds(my_rows, HALF), :]
     norm_copy = begin(remote(mine, mine, norm_sem.at[0], norm_sem.at[1], partner))
 
-    def slot(zs, xs, cs):
-        return kv_buf.at[zs, pl.ds(pl.multiple_of((xs * 2 + cs) * HALF, HALF), HALF), :]
-
-    def slot_half(zs, xs, cs, part):
+    blocks = (k_buf, v_buf)
+
+    def slot(kind, zs, xs, cs):
+        return blocks[kind].at[zs, pl.ds(pl.multiple_of((xs * 2 + cs) * HALF, HALF), HALF), :]
+
+    def slot_half(kind, zs, xs, cs, part):
         start = pl.multiple_of((xs * 2 + cs) * HALF + part * (HALF // 2), HALF // 2)
-        return kv_buf.at[zs, pl.ds(start, HALF // 2), :]
+        return blocks[kind].at[zs, pl.ds(start, HALF // 2), :]
 
     u = z % 4
     ranks = (u, u + 1 - 2 * (u % 2), 2 - u // 2, 3 * (1 - u // 2))
     same = 1 - src_tp - c + 2 * src_tp * c
     z_sends = []
 
-    def z_send(rank, half, index):
-        head = same * ranks[rank] + (1 - same) * ranks[3 - rank]
-        target = 4 * c + head
-        device = {"sp": target * NX + x, "tp": half}
-        kv_copy = remote(
-            kv_send.at[head, half], slot(z, x, half), kv_ss.at[index], kv_rs.at[z], device
-        )
-        q_copy = remote(q_send.at[head, half], q_raw.at[z], q_ss.at[index], q_rs.at[z], device)
-        away = jnp.logical_not((target == z) & (half == c))
-        z_sends.append((away, kv_copy, q_copy))
-
-        @pl.when(away)
-        def _():
-            kv_copy.start()
-            q_copy.start()
+    sources = (k_send, v_send, q_send)
+
+    def z_send(kind, half, base):
+        for rank in range(4):
+            head = same * ranks[rank] + (1 - same) * ranks[3 - rank]
+            target = 4 * c + head
+            landing = q_raw.at[z] if kind == 2 else slot(kind, z, x, half)
+            copy = remote(
+                sources[kind].at[head, half],
+                landing,
+                z_ss.at[kind, base + rank],
+                z_rs.at[kind, z],
+                {"sp": target * NX + x, "tp": half},
+            )
+            away = jnp.logical_not((target == z) & (half == c))
+            z_sends.append((away, copy))
+
+            @pl.when(away)
+            def _(copy=copy):
+                copy.start()
 
     z_send(0, c, 0)
-    z_send(1, c, 1)
+    project_values(my_rows, c, True)
 
     @pl.when(local)
     def _():
-        kv_buf[z, pl.ds(pl.multiple_of((x * 2 + c) * HALF, HALF), HALF), :] = kv_send[own_head, c]
-        q_raw[z] = q_send[own_head, c]
+        mine = pl.ds(pl.multiple_of((x * 2 + c) * HALF, HALF), HALF)
+        k_buf[z, mine, :] = k_send[own_head, c]
+        v_buf[z, mine, :] = v_send[own_head, c]
 
     w_hbm = (woc_hbm, woa_hbm)
 
@@ -267,16 +279,18 @@
 
     project_glu(my_rows, True)
     norm_copy.wait_recv()
-    project_qkv(peer_rows, other, False)
-    z_send(0, other, 2)
-    z_send(1, other, 3)
-    z_send(2, c, 4)
-    z_send(2, other, 5)
-    z_send(3, c, 6)
-    z_send(3, other, 7)
+    project_keys(peer_rows, other, False)
+    z_send(0, other, 4)
     project_glu(peer_rows, False)
     halo_send[...] = gated_ext[2 * HALF :, :].astype(BF16)
     halo_copy = begin(remote(halo_send, halo_recv, halo_sem.at[0], halo_sem.at[1], following))
+    project_values(peer_rows, other, False)
+    project_queries(my_rows, c, True)
+    project_queries(peer_rows, other, False)
+
+    @pl.when(local)
+    def _():
+        q_raw[z] = q_send[own_head, c]
 
     own_w = []
     for kind in range(2):
@@ -306,50 +320,55 @@
         squares = jnp.sum(total * total, axis=-1, keepdims=True)
         sums_send[base : base + 32, :] = jnp.where(low[:32], sums, squares)
 
-    def stage_one(zs):
-        ref = slot(zs, x, c)
-        away = jnp.logical_not((zs == z) & local)
-
-        @pl.when(away)
+    def z_wait(kind, zs):
+        ref = q_raw.at[zs] if kind == 2 else slot(kind, zs, x, c)
+
+        @pl.when(jnp.logical_not((zs == z) & local))
         def _():
-            remote(ref, ref, kv_ss.at[0], kv_rs.at[zs], partner).wait_recv()
-
-        begin(remote(ref, ref, xs_ss.at[0, zs], xs_rs.at[0, zs], right))
-        begin(remote(ref, ref, xs_ss.at[1, zs], xs_rs.at[1, zs], left))
-        begin(remote(ref, ref, d_ss.at[0, zs], d_rs.at[0, zs], partner))
-
-        @pl.when(away)
-        def _():
-            remote(q_raw.at[zs], q_raw.at[zs], q_ss.at[0], q_rs.at[zs], partner).wait_recv()
-
+            remote(ref, ref, z_ss.at[kind, 0], z_rs.at[kind, zs], partner).wait_recv()
+
+    def pass_on(kind, ref, arrival, device):
+        remote(ref, ref, xs_ss.at[kind], arrival, device).start()
+
+    def share(kind, ref, zs):
+        remote(ref, ref, d_ss.at[kind], d_rs.at[kind, zs], partner).start()
+
+    def arrive(kind, rows, arrival):
+        ref = blocks[kind].at[0, pl.ds(0, rows), :]
+        remote(ref, ref, xs_ss.at[kind], arrival, partner).wait_recv()
+
+    def stage_one(kind, zs):
+        ref = slot(kind, zs, x, c)
+        pass_on(kind, ref, xs_rs.at[kind, 0, zs], right)
+        pass_on(kind, ref, xs_rs.at[kind, 0, zs], left)
+        share(kind, ref, zs)
+
+    def stage_queries(zs):
+        z_wait(2, zs)
         rows = q_raw[zs]
         zero = jnp.zeros_like(rows)
         qs[zs, :HALF] = jnp.where(low, rows, zero)
         qs[zs, HALF:] = jnp.where(low, zero, rows)
 
-    def stage_two(zs):
-        ref = slot(zs, xl, c)
-        remote(ref, ref, xs_ss.at[0, zs], xs_rs.at[0, zs], right).wait_recv()
-        part = slot_half(zs, xl, c, 0)
-        begin(remote(part, part, xs_ss.at[2, zs], xs_rs.at[2, zs], right))
-        begin(remote(ref, ref, d_ss.at[1, zs], d_rs.at[1, zs], partner))
-        ref = slot(zs, xr, c)
-        remote(ref, ref, xs_ss.at[1, zs], xs_rs.at[1, zs], left).wait_recv()
-        part = slot_half(zs, xr, c, 1)
-        begin(remote(part, part, xs_ss.at[3, zs], xs_rs.at[3, zs], left))
-        begin(remote(ref, ref, d_ss.at[2, zs], d_rs.at[2, zs], partner))
-
-    def stage_three(zs):
-        for part in range(2):
-            ref = slot_half(zs, xo, c, part)
-            remote(ref, ref, xs_ss.at[2 + part, zs], xs_rs.at[2 + part, zs], right).wait_recv()
-        ref = slot(zs, xo, c)
-        begin(remote(ref, ref, d_ss.at[3, zs], d_rs.at[3, zs], partner))
-
-    def stage_four(zs):
-        for relation, xs in enumerate((x, xl, xr, xo)):
-            ref = slot(zs, xs, other)
-            remote(ref, ref, d_ss.at[relation, zs], d_rs.at[relation, zs], partner).wait_recv()
+    def stage_two(kind, zs):
+        arrive(kind, 2 * HALF, xs_rs.at[kind, 0, zs])
+        pass_on(kind, slot_half(kind, zs, xl, c, 0), xs_rs.at[kind, 1, zs], right)
+        pass_on(kind, slot_half(kind, zs, xr, c, 1), xs_rs.at[kind, 1, zs], left)
+        share(kind, slot(kind, zs, xl, c), zs)
+        share(kind, slot(kind, zs, xr, c), zs)
+
+    def stage_three(kind, zs):
+        arrive(kind, HALF, xs_rs.at[kind, 1, zs])
+        share(kind, slot(kind, zs, xo, c), zs)
+
+    def stage_four(kind, zs):
+        arrive(kind, 4 * HALF, d_rs.at[kind, zs])
+
+    def sent_all(kind):
+        ref = blocks[kind].at[pl.ds(0, 3)]
+        remote(ref, ref, xs_ss.at[kind], d_rs.at[0, 0], partner).wait_send()
+        ref = blocks[kind].at[pl.ds(0, 4)]
+        remote(ref, ref, d_ss.at[kind], d_rs.at[0, 0], partner).wait_send()
 
     def w_wait(source, kind, side):
         ref = w_buf.at[source, c, kind]
@@ -449,13 +468,16 @@
         offset = odd * ((index + 1) // 2) + (1 - odd) * (NZ - index // 2)
         return (z + offset) % NZ
 
+    before = (z * (z + 1)) // 2
+
     def which(t):
+        skipped = t + jnp.where(t >= before, z + 1, 0)
+        t = jnp.where(t >= 35 - z, t - 35 + z + before, skipped)
         i = 0
         for bound in (1, 3, 6, 10, 15, 21, 28):
             i = i + jnp.where(t >= bound, 1, 0)
         j = t - (i * (i + 1)) // 2
-        zi, zj = place(i), place(j)
-        return jnp.minimum(zi, zj), jnp.maximum(zi, zj), (j + 1) // (i + 1)
+        return j, i, (j + 1) // (i + 1)
 
     def scores(t, score_ref, max_ref):
         s, zt, kind = which(t)
@@ -463,7 +485,7 @@
         best = None
         for start in range(0, 1024, 256):
             block = lax.dot_general(
-                kv_buf[s, start : start + 256, 0:128],
+                k_buf[s, start : start + 256, :],
                 queries,
                 (((1,), (1,)), ((), ())),
                 preferred_element_type=F32,
@@ -495,8 +517,8 @@
                 [
                     jnp.concatenate(
                         [
-                            kv_buf[s, start : start + 128, 128:256],
-                            kv_buf[s, start + 128 : start + 256, 128:256],
+                            v_buf[s, start : start + 128, :],
+                            v_buf[s, start + 128 : start + 256, :],
                         ],
                         axis=1,
                     ),
@@ -511,7 +533,7 @@
 
     def ret_copy(s):
         return remote(
-            ret_send.at[s], attn_buf.at[z], ret_ss.at[s], ret_rs.at[z], {"sp": s * NX + x}
+            ret_send.at[s], attn_buf.at[z], ret_ss, ret_rs.at[z], {"sp": s * NX + x}
         )
 
     def log_copy(s):
@@ -553,76 +575,94 @@
         def _():
             log_copy(s).start()
 
+    def finish_one_of(t):
+        _, first, first_done = which(t)
+        _, second, second_done = which(t + 1)
+
+        def run(_, carry):
+            finish(first * first_done + second * second_done)
+            return carry
+
+        lax.fori_loop(0, first_done + second_done, run, 0)
+
     def pair(p, carry):
         scores(2 * p + 1, score_b, max_b)
         absorb(2 * p, score_a, max_a)
         scores(2 * p + 2, score_a, max_a)
         absorb(2 * p + 1, score_b, max_b)
+        finish_one_of(2 * p)
         return carry
 
-    last = place(NZ - 1)
-    conv_copy = None
+    for part in (1, 2, 3, 4, 5, 6, 7):
+        conv_chunk(part)
+    for step in range(NZ):
+        z_wait(0, place(step))
+        stage_one(0, place(step))
+        if step == Z_GATE:
+            z_send(1, c, 0)
+            z_send(1, other, 4)
+    for step in range(NZ):
+        stage_two(0, place(step))
+    for step in range(NZ):
+        z_wait(1, place(step))
+        if step == Z_GATE:
+            z_send(2, c, 0)
+            z_send(2, other, 4)
+    for step in range(V_SPLIT):
+        stage_one(1, step)
+    w_one()
+    for step in range(NZ):
+        stage_three(0, place(step))
+    halo_copy.wait_recv()
+    rows = halo_recv[...].astype(F32)
+    gated_ext[0:32, :] = jnp.where(me == 0, jnp.zeros_like(rows), rows)
+    conv_chunk(0)
+    sums_copy = begin(remote(sums_send, sums_recv, sums_sem.at[0], sums_sem.at[1], partner))
+    for step in range(NZ):
+        stage_four(0, place(step))
+    for step in range(V_SPLIT):
+        stage_two(1, step)
+    for step in range(V_SPLIT, NZ):
+        stage_one(1, step)
+    conv_copy = conv_finish()
+    for step in range(V_SPLIT):
+        stage_three(1, step)
+    lam_copy.wait_recv()
+    stage_queries(0)
+    stage_four(1, 0)
     done_pairs = 0
-    for step in range(NZ + 2):
-        if step < NZ:
-            stage_one(place(step))
-        if step == 0:
-            for part in (1, 2, 3, 4, 5, 6, 7):
-                conv_chunk(part)
-            halo_copy.wait_recv()
-            rows = halo_recv[...].astype(F32)
-            gated_ext[0:32, :] = jnp.where(me == 0, jnp.zeros_like(rows), rows)
-            conv_chunk(0)
-            sums_copy = begin(remote(sums_send, sums_recv, sums_sem.at[0], sums_sem.at[1], partner))
-        if 0 <= step - 1 < NZ:
-            stage_two(place(step - 1))
-        if step == 2:
-            conv_copy = conv_finish()
-        if step == NZ + 1:
-            lam_copy.wait_recv()
-
-            def early(j, carry):
-                zj = place(j)
-
-                @pl.when(zj < last)
-                def _():
-                    finish(zj)
-
-                return carry
-
-            lax.fori_loop(0, 5, early, 0)
-        if 0 <= step - 2 < NZ:
-            stage_three(place(step - 2))
-        if step == W_ONE:
-            w_one()
-        if step == W_TWO:
+    for index in range(NZ):
+        if index + 1 < NZ:
+            stage_queries(index + 1)
+            stage_four(1, index + 1)
+        if index == 0:
+            scores(0, score_a, max_a)
+        else:
+            end = ((index + 1) * (index + 2) // 2 - 1) // 2
+            lax.fori_loop(done_pairs, end, pair, 0)
+            done_pairs = end
+        if index == V_SPLIT - 3:
+            for step in range(V_SPLIT, NZ):
+                stage_two(1, step)
             w_two()
-        if 0 <= step - 2 < NZ:
-            index = step - 2
-            stage_four(place(index))
-            if index == 0:
-                scores(0, score_a, max_a)
-            else:
-                end = ((index + 1) * (index + 2) // 2 - 1) // 2
-                lax.fori_loop(done_pairs, end, pair, 0)
-                done_pairs = end
+        if index == V_SPLIT - 2:
+            for step in range(V_SPLIT, NZ):
+                stage_three(1, step)
+        if index == W_THREE:
+            w_three()
+    w_four()
     scores(35, score_b, max_b)
     absorb(34, score_a, max_a)
     absorb(35, score_b, max_b)
 
-    def late(j, carry):
-        zj = place(j)
-
-        @pl.when((j > 4) | (zj > last))
-        def _():
-            finish(zj)
-
+    def run_last(_, carry):
+        finish(NZ - 1)
         return carry
 
-    lax.fori_loop(0, NZ, late, 0)
-
-    w_three()
-    w_four()
+    lax.fori_loop(0, (7 - z) // 7, run_last, 0)
+
+    finish(z)
+
     for kind in range(2):
         own_w[kind].wait()
     conv_copy.wait_recv()
@@ -639,7 +679,7 @@
         @pl.when(hs != z)
         def _(hs=hs):
             remote(
-                attn_buf.at[hs], attn_buf.at[hs], ret_ss.at[hs], ret_rs.at[hs], partner
+                attn_buf.at[hs], attn_buf.at[hs], ret_ss, ret_rs.at[hs], partner
             ).wait_recv()
 
     sides = [jnp.concatenate([attn_buf[4 * side + k] for k in range(4)], axis=1) for side in range(2)]
@@ -666,24 +706,28 @@
                     head, half, which_map : which_map + 1, :
                 ]
 
-    for away, kv_copy, q_copy in z_sends:
+    for away, copy in z_sends:
 
         @pl.when(away)
-        def _(kv_copy=kv_copy, q_copy=q_copy):
-            kv_copy.wait_send()
-            q_copy.wait_send()
+        def _(copy=copy):
+            copy.wait_send()
 
     for copy in pending:
         copy.wait_send()
+    sent_all(0)
+    sent_all(1)
+    ref = ret_send.at[pl.ds(0, NZ - 1)]
+    remote(ref, ref, ret_ss, ret_rs.at[0], partner).wait_send()
     for s in range(NZ):
-
-        @pl.when(s != z)
-        def _(s=s):
-            ret_copy(s).wait_send()
 
         @pl.when(jnp.logical_not((s == z) & local))
         def _(s=s):
             log_copy(s).wait_send()
+
+
+def hand_over(mixed_ref, logs_ref, mixed_out, logs_out):
+    mixed_out[...] = mixed_ref[...]
+    logs_out[...] = logs_ref[...]
 
 
 def body(
@@ -723,9 +767,11 @@
             pltpu.VMEM((D, 256), BF16),
             pltpu.VMEM((D, 512), BF16),
             pltpu.VMEM((2 * HALF, D), BF16),
-            pltpu.VMEM((4, 2, HALF, 256), BF16),
             pltpu.VMEM((4, 2, HALF, 128), BF16),
-            pltpu.VMEM((NZ, NX * 2 * HALF, 256), BF16),
+            pltpu.VMEM((4, 2, HALF, 128), BF16),
+            pltpu.VMEM((4, 2, HALF, 128), BF16),
+            pltpu.VMEM((NZ, NX * 2 * HALF, 128), BF16),
+            pltpu.VMEM((NZ, NX * 2 * HALF, 128), BF16),
             pltpu.VMEM((NZ, HALF, 128), BF16),
             pltpu.VMEM((NZ, 2 * HALF, 128), BF16),
             pltpu.VMEM((2 * HALF + 32, 512), F32),
@@ -754,19 +800,17 @@
             pltpu.VMEM((HALF, D), F32),
             dma((7,)),
             dma((2,)),
-            dma((8,)),
-            dma((8,)),
-            dma((NZ,)),
-            dma((NZ,)),
-            dma((4, NZ)),
-            dma((4, NZ)),
-            dma((4, NZ)),
-            dma((4, NZ)),
+            dma((3, 8)),
+            dma((3, NZ)),
+            dma((2,)),
+            dma((2, 2, NZ)),
+            dma((2,)),
+            dma((2, NZ)),
             dma((2,)),
             dma((2,)),
             dma((2,)),
             dma((2,)),
-            dma((NZ,)),
+            dma,
             dma((NZ,)),
             dma((NZ,)),
             dma((4, 2)),
@@ -801,6 +845,16 @@
         w_out_conv,
         w_out_attn,
     )
+    mixed, logs = pl.pallas_call(
+        hand_over,
+        out_shape=(
+            jax.ShapeDtypeStruct((HALF, D), BF16),
+            jax.ShapeDtypeStruct((2, 4, 2 * HALF), F32),
+        ),
+        in_specs=[vmem, vmem],
+        out_specs=(vmem, vmem),
+        name="hand_over",
+    )(mixed, logs)
     return (mixed[None], logs[None])
 
 

time: 81.4 us -> 61.8 us (0.76)
  Pallas kernels: 77.4 us -> 61 us
  local copies, waits for them, and re-layouts: 3.18 us -> 0 us
    pallas_call x1, Pallas kernels: 77.4 us -> 59.1 us  [body(): pl.pallas_call(kernel, out_shape=(jax.ShapeDtypeStruct((HALF, D), BF16),...]
    unnamed x2 -> x0, local copies, waits for them, and re-layouts: 3.18 us -> none
    pallas_call x0 -> x1, Pallas kernels: none -> 1.87 us  [body(): pl.pallas_call(hand_over, out_shape=(jax.ShapeDtypeStruct((HALF, D), BF16...]
where the time goes in v3:
time: 61.8 us; the launch traced here: 61.6 us
  Pallas kernels  61 us (99%)
  between operations  0.64 us (1%)
    pallas_call x1, Pallas kernels, body(): pl.pallas_call(kernel, out_shape=(jax.ShapeDtypeStruct((HALF, D), BF16),...  59.1 us
    pallas_call x1, Pallas kernels, body(): pl.pallas_call(hand_over, out_shape=(jax.ShapeDtypeStruct((HALF, D), BF16...  1.87 us

profile of v3, /device:TPU:1, one launch (start us, length us, event | category | flops | bytes accessed | tf_op | source)
XLA Modules:
  0.0 61.6 jit_solution(6859724128413049032)
XLA Ops:
  0.6 59.1 %mixer.1 = (bf16[128,2048]{1,0:T(8,128)(2,1)}, f32[2,4,256]{2,1,0:T(4,128)}) custom-call(bf16[128,2048]{1,0:T(8,128)(2,1)} %bitcast.6, f32[1,2048]{1,0:T(1,128)} %bitcast.7, bf16[31,512]{1,0:T(8,128)(2,1)} %ck_ref.1, f32[1,512]{1,0:T(1,128)} %bitcast.8, f32[1,128]{1,0:T(1,128)} %bitcast.9, f32[4]{0:T(128)} %lam_ref.1, bf16[2048,512]{1,0:T(8,128)(2,1)} %wgv_hbm.1, ...), custom_call_target="tpu_custom_call" | custom-call | tf_op jit(solution)/shard_map/mixer/pallas_call | solution.py:753
  59.8 1.9 %hand_over.1 = (bf16[128,2048]{1,0:T(8,128)(2,1)}, f32[2,4,256]{2,1,0:T(4,128)}) custom-call(bf16[128,2048]{1,0:T(8,128)(2,1)} %get-tuple-element.6.mixed_ref, f32[2,4,256]{2,1,0:T(4,128)} %get-tuple-element.7.logs_ref), custom_call_target="tpu_custom_call" | custom-call | tf_op jit(solution)/shard_map/hand_over/pallas_call | solution.py:848

commit v4 on v3

--- a/solution.py
+++ b/solution.py
@@ -13,8 +13,10 @@
 NX = 4
 NY = 4
 HALF = 128
-Z_GATE = 2
-V_SPLIT = 5
+Z_GATE = 0
+Q_GATE = 4
+FAR_FIRST = (0, 4, 5, 3, 6, 2, 7, 1)
+V_SPLIT = 4
 W_THREE = 5
 NEG_FILL = -1e30
 EPSILON = 1e-05
@@ -110,12 +112,8 @@
     log_rs,
     w_ss,
     w_rs,
-    wx_ss,
     wx_rs,
-    wd_ss,
     wd_rs,
-    wp_ss,
-    wp_rs,
     own_sem,
 ):
     me = lax.axis_index("sp")
@@ -236,30 +234,28 @@
     u = z % 4
     ranks = (u, u + 1 - 2 * (u % 2), 2 - u // 2, 3 * (1 - u // 2))
     same = 1 - src_tp - c + 2 * src_tp * c
-    z_sends = []
 
     sources = (k_send, v_send, q_send)
 
-    def z_send(kind, half, base):
-        for rank in range(4):
+    def z_send(kind, half):
+        for rank in (3, 2, 1, 0):
             head = same * ranks[rank] + (1 - same) * ranks[3 - rank]
             target = 4 * c + head
             landing = q_raw.at[z] if kind == 2 else slot(kind, z, x, half)
             copy = remote(
                 sources[kind].at[head, half],
                 landing,
-                z_ss.at[kind, base + rank],
+                z_ss.at[kind],
                 z_rs.at[kind, z],
                 {"sp": target * NX + x, "tp": half},
             )
             away = jnp.logical_not((target == z) & (half == c))
-            z_sends.append((away, copy))
 
             @pl.when(away)
             def _(copy=copy):
                 copy.start()
 
-    z_send(0, c, 0)
+    z_send(0, c)
     project_values(my_rows, c, True)
 
     @pl.when(local)
@@ -268,10 +264,33 @@
         k_buf[z, mine, :] = k_send[own_head, c]
         v_buf[z, mine, :] = v_send[own_head, c]
 
+    def z_wait(kind, zs):
+        ref = q_raw.at[zs] if kind == 2 else slot(kind, zs, x, c)
+
+        @pl.when(jnp.logical_not((zs == z) & local))
+        def _():
+            remote(ref, ref, z_ss.at[kind], z_rs.at[kind, zs], partner).wait_recv()
+
+    def pass_on(kind, ref, arrival, device):
+        remote(ref, ref, xs_ss.at[kind], arrival, device).start()
+
+    def share(kind, ref, zs):
+        remote(ref, ref, d_ss.at[kind], d_rs.at[kind, zs], partner).start()
+
+    def arrive(kind, rows, arrival):
+        ref = blocks[kind].at[0, pl.ds(0, rows), :]
+        remote(ref, ref, xs_ss.at[kind], arrival, partner).wait_recv()
+
+    def stage_one(kind, zs):
+        ref = slot(kind, zs, x, c)
+        pass_on(kind, ref, xs_rs.at[kind, 0, zs], right)
+        pass_on(kind, ref, xs_rs.at[kind, 0, zs], left)
+        share(kind, ref, zs)
+
     w_hbm = (woc_hbm, woa_hbm)
 
     def w_own(side, kind, device):
-        begin(remote(w_hbm[kind], w_buf.at[y, c, kind], w_ss.at[side, kind], w_rs.at[side, kind], device))
+        remote(w_hbm[kind], w_buf.at[y, c, kind], w_ss, w_rs.at[side, kind], device).start()
 
     w_own(0, 0, up)
     w_own(1, 1, down)
@@ -280,11 +299,13 @@
     project_glu(my_rows, True)
     norm_copy.wait_recv()
     project_keys(peer_rows, other, False)
-    z_send(0, other, 4)
+    z_send(0, other)
     project_glu(peer_rows, False)
     halo_send[...] = gated_ext[2 * HALF :, :].astype(BF16)
     halo_copy = begin(remote(halo_send, halo_recv, halo_sem.at[0], halo_sem.at[1], following))
     project_values(peer_rows, other, False)
+    z_wait(0, z)
+    stage_one(0, z)
     project_queries(my_rows, c, True)
     project_queries(peer_rows, other, False)
 
@@ -297,7 +318,7 @@
         own = pltpu.make_async_copy(w_hbm[kind], w_buf.at[y, c, kind], own_sem.at[kind])
         own.start()
         own_w.append(own)
-        begin(remote(w_hbm[kind], w_buf.at[y, c, kind], wd_ss.at[0, kind], wd_rs.at[0, kind], partner))
+        remote(w_hbm[kind], w_buf.at[y, c, kind], w_ss, wd_rs.at[kind], partner).start()
 
     taps = ck_ref[...].astype(F32)
 
@@ -320,29 +341,6 @@
         squares = jnp.sum(total * total, axis=-1, keepdims=True)
         sums_send[base : base + 32, :] = jnp.where(low[:32], sums, squares)
 
-    def z_wait(kind, zs):
-        ref = q_raw.at[zs] if kind == 2 else slot(kind, zs, x, c)
-
-        @pl.when(jnp.logical_not((zs == z) & local))
-        def _():
-            remote(ref, ref, z_ss.at[kind, 0], z_rs.at[kind, zs], partner).wait_recv()
-
-    def pass_on(kind, ref, arrival, device):
-        remote(ref, ref, xs_ss.at[kind], arrival, device).start()
-
-    def share(kind, ref, zs):
-        remote(ref, ref, d_ss.at[kind], d_rs.at[kind, zs], partner).start()
-
-    def arrive(kind, rows, arrival):
-        ref = blocks[kind].at[0, pl.ds(0, rows), :]
-        remote(ref, ref, xs_ss.at[kind], arrival, partner).wait_recv()
-
-    def stage_one(kind, zs):
-        ref = slot(kind, zs, x, c)
-        pass_on(kind, ref, xs_rs.at[kind, 0, zs], right)
-        pass_on(kind, ref, xs_rs.at[kind, 0, zs], left)
-        share(kind, ref, zs)
-
     def stage_queries(zs):
         z_wait(2, zs)
         rows = q_raw[zs]
@@ -370,68 +368,54 @@
         ref = blocks[kind].at[pl.ds(0, 4)]
         remote(ref, ref, d_ss.at[kind], d_rs.at[0, 0], partner).wait_send()
 
-    def w_wait(source, kind, side):
-        ref = w_buf.at[source, c, kind]
-        remote(ref, ref, w_ss.at[side, kind], w_rs.at[side, kind], up).wait_recv()
-
-    def w_share(source, kind, relation):
-        ref = w_buf.at[source, c, kind]
-        begin(remote(ref, ref, wd_ss.at[relation, kind], wd_rs.at[relation, kind], partner))
+    def w_wait(ref, arrival):
+        remote(ref, ref, w_ss, arrival, partner).wait_recv()
+
+    def w_pass(ref, arrival, device):
+        remote(ref, ref, w_ss, arrival, device).start()
 
     def piece(source, core, kind, xs):
         return w_buf.at[source, core, kind, pl.ds(pl.multiple_of(xs * 128, 128), 128), :]
 
-    def piece_share(kind, relation, xs):
-        ref = piece(yo, c, kind, xs)
-        begin(remote(ref, ref, wp_ss.at[relation, kind], wp_rs.at[relation, kind], partner))
-
     def w_one():
-        w_wait(yl, 0, 0)
-        ref = piece(yl, c, 0, x)
-        begin(remote(ref, ref, w_ss.at[2, 0], w_rs.at[2, 0], up))
+        w_wait(w_buf.at[yl, c, 0], w_rs.at[0, 0])
+        w_pass(piece(yl, c, 0, x), w_rs.at[2, 0], up)
         w_own(0, 1, up)
-        w_wait(yr, 1, 1)
-        ref = piece(yr, c, 1, x)
-        begin(remote(ref, ref, w_ss.at[2, 1], w_rs.at[2, 1], down))
+        w_wait(w_buf.at[yr, c, 1], w_rs.at[1, 1])
+        w_pass(piece(yr, c, 1, x), w_rs.at[2, 1], down)
         w_own(1, 0, down)
-        w_share(yl, 0, 1)
-        w_share(yr, 1, 2)
+        w_pass(w_buf.at[yl, c, 0], wd_rs.at[0], partner)
+        w_pass(w_buf.at[yr, c, 1], wd_rs.at[1], partner)
 
     def w_two():
         for kind in range(2):
             ref = piece(yo, c, kind, x)
-            remote(ref, ref, w_ss.at[2, kind], w_rs.at[2, kind], up).wait_recv()
-            begin(remote(ref, ref, wx_ss.at[0, kind], wx_rs.at[0, kind], right))
-            begin(remote(ref, ref, wx_ss.at[1, kind], wx_rs.at[1, kind], left))
-            piece_share(kind, 0, x)
+            w_wait(ref, w_rs.at[2, kind])
+            w_pass(ref, wx_rs.at[0, kind], right)
+            w_pass(ref, wx_rs.at[1, kind], left)
+            w_pass(ref, wd_rs.at[kind], partner)
 
     def w_three():
         for kind in range(2):
             for side, xs in ((0, xl), (1, xr)):
                 ref = piece(yo, c, kind, xs)
-                remote(ref, ref, wx_ss.at[side, kind], wx_rs.at[side, kind], right).wait_recv()
+                w_wait(ref, wx_rs.at[side, kind])
                 if side == kind:
-                    device = right if side == 0 else left
-                    begin(remote(ref, ref, wx_ss.at[2, kind], wx_rs.at[2, kind], device))
-                piece_share(kind, 1 + side, xs)
+                    w_pass(ref, wx_rs.at[2, kind], right if side == 0 else left)
+                w_pass(ref, wd_rs.at[kind], partner)
 
     def w_four():
-        w_wait(yl, 1, 0)
-        w_share(yl, 1, 1)
-        w_wait(yr, 0, 1)
-        w_share(yr, 0, 2)
-        for kind in range(2):
-            ref = piece(yo, c, kind, xo)
-            remote(ref, ref, wx_ss.at[2, kind], wx_rs.at[2, kind], right).wait_recv()
-            piece_share(kind, 3, xo)
+        w_wait(w_buf.at[yr, c, 0], w_rs.at[1, 0])
+        w_pass(w_buf.at[yr, c, 0], wd_rs.at[0], partner)
+        w_wait(piece(yo, c, 0, xo), wx_rs.at[2, 0])
+        w_pass(piece(yo, c, 0, xo), wd_rs.at[0], partner)
+        w_wait(w_buf.at[yl, c, 1], w_rs.at[0, 1])
+        w_pass(w_buf.at[yl, c, 1], wd_rs.at[1], partner)
+        w_wait(piece(yo, c, 1, xo), wx_rs.at[2, 1])
+        w_pass(piece(yo, c, 1, xo), wd_rs.at[1], partner)
 
     def w_five(kind):
-        for relation, source in enumerate((y, yl, yr)):
-            ref = w_buf.at[source, other, kind]
-            remote(ref, ref, wd_ss.at[relation, kind], wd_rs.at[relation, kind], partner).wait_recv()
-        for relation, xs in enumerate((x, xl, xr, xo)):
-            ref = piece(yo, other, kind, xs)
-            remote(ref, ref, wp_ss.at[relation, kind], wp_rs.at[relation, kind], partner).wait_recv()
+        w_wait(w_buf.at[0], wd_rs.at[kind])
 
     def conv_finish():
         sums_copy.wait_recv()
@@ -464,9 +448,7 @@
     gain_t[...] = jnp.transpose(jnp.broadcast_to(hg_ref[...], (128, 128))) * HEAD_SCALE
 
     def place(index):
-        odd = index % 2
-        offset = odd * ((index + 1) // 2) + (1 - odd) * (NZ - index // 2)
-        return (z + offset) % NZ
+        return (z + FAR_FIRST[index]) % NZ
 
     before = (z * (z + 1)) // 2
 
@@ -533,12 +515,12 @@
 
     def ret_copy(s):
         return remote(
-            ret_send.at[s], attn_buf.at[z], ret_ss, ret_rs.at[z], {"sp": s * NX + x}
+            ret_send.at[s], attn_buf.at[z], ret_ss, ret_rs, {"sp": s * NX + x}
         )
 
     def log_copy(s):
         return remote(
-            lsend.at[s], log_buf.at[own_head, c], log_ss.at[s], log_rs.at[own_head, c],
+            lsend.at[s], log_buf.at[own_head, c], log_ss, log_rs,
             {"sp": s * NX + x, "tp": src_tp},
         )
 
@@ -593,21 +575,22 @@
         finish_one_of(2 * p)
         return carry
 
-    for part in (1, 2, 3, 4, 5, 6, 7):
-        conv_chunk(part)
     for step in range(NZ):
-        z_wait(0, place(step))
-        stage_one(0, place(step))
+        if step > 0:
+            z_wait(0, place(step))
+            stage_one(0, place(step))
         if step == Z_GATE:
-            z_send(1, c, 0)
-            z_send(1, other, 4)
+            z_send(1, c)
+            z_send(1, other)
     for step in range(NZ):
         stage_two(0, place(step))
+        if step > 0:
+            conv_chunk(step)
+        if step == Q_GATE:
+            z_send(2, c)
+            z_send(2, other)
     for step in range(NZ):
         z_wait(1, place(step))
-        if step == Z_GATE:
-            z_send(2, c, 0)
-            z_send(2, other, 4)
     for step in range(V_SPLIT):
         stage_one(1, step)
     w_one()
@@ -618,8 +601,6 @@
     gated_ext[0:32, :] = jnp.where(me == 0, jnp.zeros_like(rows), rows)
     conv_chunk(0)
     sums_copy = begin(remote(sums_send, sums_recv, sums_sem.at[0], sums_sem.at[1], partner))
-    for step in range(NZ):
-        stage_four(0, place(step))
     for step in range(V_SPLIT):
         stage_two(1, step)
     for step in range(V_SPLIT, NZ):
@@ -628,6 +609,8 @@
     for step in range(V_SPLIT):
         stage_three(1, step)
     lam_copy.wait_recv()
+    for step in range(NZ):
+        stage_four(0, place(step))
     stage_queries(0)
     stage_four(1, 0)
     done_pairs = 0
@@ -644,10 +627,10 @@
         if index == V_SPLIT - 3:
             for step in range(V_SPLIT, NZ):
                 stage_two(1, step)
-            w_two()
         if index == V_SPLIT - 2:
             for step in range(V_SPLIT, NZ):
                 stage_three(1, step)
+            w_two()
         if index == W_THREE:
             w_three()
     w_four()
@@ -674,13 +657,8 @@
         ) + jnp.dot(conv_full[1], w_buf[quarter, 1, 0], preferred_element_type=F32)
     w_five(1)
 
-    for hs in range(NZ):
-
-        @pl.when(hs != z)
-        def _(hs=hs):
-            remote(
-                attn_buf.at[hs], attn_buf.at[hs], ret_ss, ret_rs.at[hs], partner
-            ).wait_recv()
+    ref = ret_send.at[pl.ds(0, NZ - 1)]
+    remote(ref, ref, ret_ss, ret_rs, partner).wait_recv()
 
     sides = [jnp.concatenate([attn_buf[4 * side + k] for k in range(4)], axis=1) for side in range(2)]
     for quarter in range(NY):
@@ -692,37 +670,36 @@
             )
         out_ref[:, cols] = result.astype(BF16)
 
+    for condition, count in ((local, 7), (jnp.logical_not(local), 8)):
+
+        @pl.when(condition)
+        def _(count=count):
+            ref = lsend.at[pl.ds(0, count)]
+            remote(ref, ref, log_ss, log_rs, partner).wait()
+
     for head in range(4):
         for half in range(2):
-            from_self = (4 * c + head == z) & (c == half)
-
-            @pl.when(jnp.logical_not(from_self))
-            def _(head=head, half=half):
-                ref = log_buf.at[head, half]
-                remote(ref, ref, log_ss.at[0], log_rs.at[head, half], partner).wait_recv()
-
             for which_map in range(2):
                 log_ref[which_map, head : head + 1, half * HALF : half * HALF + HALF] = log_buf[
                     head, half, which_map : which_map + 1, :
                 ]
 
-    for away, copy in z_sends:
-
-        @pl.when(away)
-        def _(copy=copy):
-            copy.wait_send()
+    for kind in range(3):
+        for condition, count in ((local, 7), (jnp.logical_not(local), 8)):
+
+            @pl.when(condition)
+            def _(kind=kind, count=count):
+                ref = k_buf.at[0, pl.ds(0, HALF * count), :]
+                remote(ref, ref, z_ss.at[kind], z_rs.at[0, 0], partner).wait_send()
 
     for copy in pending:
         copy.wait_send()
     sent_all(0)
     sent_all(1)
     ref = ret_send.at[pl.ds(0, NZ - 1)]
-    remote(ref, ref, ret_ss, ret_rs.at[0], partner).wait_send()
-    for s in range(NZ):
-
-        @pl.when(jnp.logical_not((s == z) & local))
-        def _(s=s):
-            log_copy(s).wait_send()
+    remote(ref, ref, ret_ss, ret_rs, partner).wait_send()
+    ref = w_buf.at[:, :, :, pl.ds(0, 448), :]
+    remote(ref, ref, w_ss, w_rs.at[0, 0], partner).wait_send()
 
 
 def hand_over(mixed_ref, logs_ref, mixed_out, logs_out):
@@ -800,7 +777,7 @@
             pltpu.VMEM((HALF, D), F32),
             dma((7,)),
             dma((2,)),
-            dma((3, 8)),
+            dma((3,)),
             dma((3, NZ)),
             dma((2,)),
             dma((2, 2, NZ)),
@@ -811,17 +788,13 @@
             dma((2,)),
             dma((2,)),
             dma,
-            dma((NZ,)),
-            dma((NZ,)),
-            dma((4, 2)),
+            dma,
+            dma,
+            dma,
+            dma,
             dma((3, 2)),
             dma((3, 2)),
-            dma((3, 2)),
-            dma((3, 2)),
-            dma((3, 2)),
-            dma((3, 2)),
-            dma((4, 2)),
-            dma((4, 2)),
+            dma((2,)),
             dma((2,)),
         ],
         compiler_params=pltpu.CompilerParams(

time: 61.8 us -> 60.9 us (0.985)
  Pallas kernels: 61 us -> 60.1 us
    pallas_call x1, Pallas kernels: 59.1 us -> 58.3 us  [body(): pl.pallas_call(kernel, out_shape=(jax.ShapeDtypeStruct((HALF, D), BF16),...]
where the time goes in v4:
time: 60.9 us; the launch traced here: 60.8 us
  Pallas kernels  60.1 us (99%)
  between operations  0.64 us (1%)
    pallas_call x1, Pallas kernels, body(): pl.pallas_call(kernel, out_shape=(jax.ShapeDtypeStruct((HALF, D), BF16),...  58.3 us
    pallas_call x1, Pallas kernels, body(): pl.pallas_call(hand_over, out_shape=(jax.ShapeDtypeStruct((HALF, D), BF16...  1.87 us

profile of v4, /device:TPU:1, one launch (start us, length us, event | category | flops | bytes accessed | tf_op | source)
XLA Modules:
  0.0 60.8 jit_solution(6541831224171407557)
XLA Ops:
  0.6 58.3 %mixer.1 = (bf16[128,2048]{1,0:T(8,128)(2,1)}, f32[2,4,256]{2,1,0:T(4,128)}) custom-call(bf16[128,2048]{1,0:T(8,128)(2,1)} %bitcast.6, f32[1,2048]{1,0:T(1,128)} %bitcast.7, bf16[31,512]{1,0:T(8,128)(2,1)} %ck_ref.1, f32[1,512]{1,0:T(1,128)} %bitcast.8, f32[1,128]{1,0:T(1,128)} %bitcast.9, f32[4]{0:T(128)} %lam_ref.1, bf16[2048,512]{1,0:T(8,128)(2,1)} %wgv_hbm.1, ...), custom_call_target="tpu_custom_call" | custom-call | tf_op jit(solution)/shard_map/mixer/pallas_call | solution.py:730
  58.9 1.9 %hand_over.1 = (bf16[128,2048]{1,0:T(8,128)(2,1)}, f32[2,4,256]{2,1,0:T(4,128)}) custom-call(bf16[128,2048]{1,0:T(8,128)(2,1)} %get-tuple-element.6.mixed_ref, f32[2,4,256]{2,1,0:T(4,128)} %get-tuple-element.7.logs_ref), custom_call_target="tpu_custom_call" | custom-call | tf_op jit(solution)/shard_map/hand_over/pallas_call | solution.py:821

commit v5 on v4

--- a/solution.py
+++ b/solution.py
@@ -624,7 +624,7 @@
             end = ((index + 1) * (index + 2) // 2 - 1) // 2
             lax.fori_loop(done_pairs, end, pair, 0)
             done_pairs = end
-        if index == V_SPLIT - 3:
+        if index == 0:
             for step in range(V_SPLIT, NZ):
                 stage_two(1, step)
         if index == V_SPLIT - 2:

time: 60.9 us -> 60.5 us (level)
  no operation moved by 1% of the time
where the time goes in v5:
time: 60.5 us; the launch traced here: 60.4 us
  Pallas kernels  59.8 us (99%)
  between operations  0.64 us (1%)
    pallas_call x1, Pallas kernels, body(): pl.pallas_call(kernel, out_shape=(jax.ShapeDtypeStruct((HALF, D), BF16),...  57.9 us
    pallas_call x1, Pallas kernels, body(): pl.pallas_call(hand_over, out_shape=(jax.ShapeDtypeStruct((HALF, D), BF16...  1.87 us

profile of v5, /device:TPU:1, one launch (start us, length us, event | category | flops | bytes accessed | tf_op | source)
XLA Modules:
  0.0 60.4 jit_solution(8432517847583687475)
XLA Ops:
  0.6 57.9 %mixer.1 = (bf16[128,2048]{1,0:T(8,128)(2,1)}, f32[2,4,256]{2,1,0:T(4,128)}) custom-call(bf16[128,2048]{1,0:T(8,128)(2,1)} %bitcast.6, f32[1,2048]{1,0:T(1,128)} %bitcast.7, bf16[31,512]{1,0:T(8,128)(2,1)} %ck_ref.1, f32[1,512]{1,0:T(1,128)} %bitcast.8, f32[1,128]{1,0:T(1,128)} %bitcast.9, f32[4]{0:T(128)} %lam_ref.1, bf16[2048,512]{1,0:T(8,128)(2,1)} %wgv_hbm.1, ...), custom_call_target="tpu_custom_call" | custom-call | tf_op jit(solution)/shard_map/mixer/pallas_call | solution.py:730
  58.5 1.9 %hand_over.1 = (bf16[128,2048]{1,0:T(8,128)(2,1)}, f32[2,4,256]{2,1,0:T(4,128)}) custom-call(bf16[128,2048]{1,0:T(8,128)(2,1)} %get-tuple-element.6.mixed_ref, f32[2,4,256]{2,1,0:T(4,128)} %get-tuple-element.7.logs_ref), custom_call_target="tpu_custom_call" | custom-call | tf_op jit(solution)/shard_map/hand_over/pallas_call | solution.py:821
